TPU v7x, 256 devices: a whole 4x4x8 slice. The times are simulated.
256 devices in a mesh: sp: 32 (over z, y), tp: 8 (over x, core).
Axes of the slice: x: 4, y: 4, z: 8, core: 2. Of those that a mesh axis runs over, the one named last changes fastest.
Arguments:
- grouped_head_inputs: bfloat16 [32768, 2, 1024], P('sp', None, 'tp'), may hold values from -6 to 6
- head_gate_inputs: bfloat16 [32768, 2, 1024], P('sp', None, 'tp'), may hold values from -6 to 6
- unsmoothed_step: float32 [32768, 2, 16], P('sp', None, 'tp'), may hold values from -3.8 to 3.8
- head_decay_rate: float32 [2, 16], P(None, 'tp'), may hold values from 3.0517578e-06 to 0.04761905
- extra_log_decay: float32 [32768, 2, 16], P('sp', None, 'tp'), may hold values from -1.4 to 0
- first_group_keys: bfloat16 [32768, 128], P('sp'), may hold values from -6 to 6
- first_group_queries: bfloat16 [32768, 128], P('sp'), may hold values from -6 to 6
- second_group_keys: bfloat16 [32768, 64], P('sp'), may hold values from -6 to 6
- second_group_queries: bfloat16 [32768, 64], P('sp'), may hold values from -6 to 6
- head_input_filter: float32 [4, 2, 1024], P(None, None, 'tp'), may hold values from -3 to 3
- first_group_filter: float32 [4, 2, 128], replicated, may hold values from -3 to 3
- second_group_filter: float32 [4, 2, 64], replicated, may hold values from -3 to 3
- head_norm_gain: float32 [2, 1024], P(None, 'tp'), may hold values from 0.1 to 1.9
- output_weight: bfloat16 [2, 1024, 2048], P(None, None, 'tp'), may hold values from -0.125 to 0.125
- residual: bfloat16 [32768, 2048], P('sp', 'tp'), may hold values from -37 to 37
- channel_norm_gain: float32 [2048], replicated, may hold values from 0.1 to 1.9
- channel_gate_weight: bfloat16 [2048, 5120], P('sp', 'tp'), may hold values from -0.125 to 0.125
- channel_up_weight: bfloat16 [2048, 5120], P('sp', 'tp'), may hold values from -0.125 to 0.125
- channel_down_weight: bfloat16 [2048, 5120], P('sp', 'tp'), may hold values from -0.078125 to 0.078125
Outputs:
- layer_output: bfloat16 [32768, 2048], P('sp', 'tp')
All inputs are finite; a program needn't handle non-finite values.
Results may differ from a plain program's by a relative error of at most 0.007.
Values may be sent and summed in bfloat16 or wider, within the bound.
A program may use at most 128 MiB of HBM per device.

v0:
```python
import jax
import jax.numpy as jnp
from jax import lax
from jax.sharding import PartitionSpec as P

HEAD = 64
CONV = 4
BLOCK = 128


EPSILON = 1e-06


def from_behind(block, axis, distance):
    devices = range(lax.axis_size(axis))
    route = [(i - distance, i) for i in devices if i - distance in devices]
    return lax.ppermute(block, axis, route)


def sent_together(arrays, axis, dim, along):
    columns = [a.reshape(*a.shape[:along], -1) for a in arrays]
    both = jnp.concatenate(columns, axis=along)
    out, at, done = (lax.all_gather(both, axis, axis=dim, tiled=True), 0, [])
    for a, column in zip(arrays, columns):
        share = out[..., at : at + column.shape[along]]
        done.append(share.reshape(*share.shape[:along], *a.shape[along:]))
        at += column.shape[along]
    return tuple(done)


def side_by_side(arrays, axis, dim, along):
    both = jnp.concatenate(arrays, axis=along)
    out, at, done = (lax.all_gather(both, axis, axis=dim, tiled=True), 0, [])
    for a in arrays:
        done.append(lax.slice_in_dim(out, at, at + a.shape[along], axis=along))
        at += a.shape[along]
    return tuple(done)


def laid_out(blocks, dim):
    shape = list(blocks.shape[1:])
    shape[dim] *= blocks.shape[0]
    return jnp.moveaxis(blocks, 0, dim).reshape(shape)


def from_everyone(x, axis):
    copies = jnp.broadcast_to(x, (lax.axis_size(axis), *x.shape))
    return lax.all_to_all(copies, axis, split_axis=0, concat_axis=0, tiled=True)


def collect(x, axis, dim):
    return laid_out(from_everyone(x, axis), dim)


def causal_taps(values, rim_values, taps):
    length = values.shape[0]
    padded = jnp.concatenate([rim_values.astype(jnp.float32), values.astype(jnp.float32)], axis=0)
    running = jnp.zeros(values.shape, jnp.float32)
    for offset in range(CONV):
        running = running + taps[offset] * padded[offset : offset + length]
    return jax.nn.silu(running)


def block_pass(current, value_rows, log_rows, key_rows, query_rows):
    cumulative = jnp.cumsum(log_rows, axis=0)
    length = value_rows.shape[0]
    causal = jnp.arange(length)[:, None] >= jnp.arange(length)[None, :]
    scores = jnp.dot(query_rows, key_rows.T)
    span_logs = jnp.where(
        causal[:, :, None], cumulative[:, None, :] - cumulative[None, :, :], -jnp.inf
    )
    weights = jnp.exp(span_logs) * scores[:, :, None]
    inside = jnp.einsum("lsh,shp->lhp", weights, value_rows)
    carried = jnp.einsum("ls,hps->lhp", query_rows, current) * jnp.exp(cumulative)[:, :, None]
    to_end = jnp.exp(cumulative[-1][None, :] - cumulative)
    update = jnp.einsum("lhp,ls->hps", value_rows * to_end[:, :, None], key_rows)
    new_state = current * jnp.exp(cumulative[-1])[:, None, None] + update
    return (new_state, inside + carried)


def scan_group(value_rows, log_rows, key_rows, query_rows):
    length, head_count, head_width = value_rows.shape
    block_count = length // BLOCK
    initial = jnp.zeros((head_count, head_width, key_rows.shape[1]), jnp.float32)
    blocks = (
        value_rows.reshape(block_count, BLOCK, head_count, head_width),
        log_rows.reshape(block_count, BLOCK, head_count),
        key_rows.reshape(block_count, BLOCK, -1),
        query_rows.reshape(block_count, BLOCK, -1),
    )

    def advance(current, pieces):
        return block_pass(current, pieces[0], pieces[1], pieces[2], pieces[3])

    final_state, outputs = lax.scan(advance, initial, blocks)
    return (final_state, outputs.reshape(length, head_count, head_width))


def shards(
    grouped_head_inputs,
    head_gate_inputs,
    unsmoothed_step,
    head_decay_rate,
    extra_log_decay,
    first_group_keys,
    first_group_queries,
    second_group_keys,
    second_group_queries,
    head_input_filter,
    first_group_filter,
    second_group_filter,
    head_norm_gain,
    output_weight,
    residual,
    channel_norm_gain,
    channel_gate_weight,
    channel_up_weight,
    channel_down_weight,
):
    rim_rows = CONV - 1
    rims = from_behind(
        (
            grouped_head_inputs[-rim_rows:],
            first_group_keys[-rim_rows:],
            first_group_queries[-rim_rows:],
            second_group_keys[-rim_rows:],
            second_group_queries[-rim_rows:],
        ),
        "sp",
        1,
    )
    conv_heads = causal_taps(grouped_head_inputs, rims[0], head_input_filter)
    keys_one = causal_taps(first_group_keys, rims[1], first_group_filter[:, 0])
    queries_one = causal_taps(first_group_queries, rims[2], first_group_filter[:, 1])
    keys_two = causal_taps(second_group_keys, rims[3], second_group_filter[:, 0])
    queries_two = causal_taps(second_group_queries, rims[4], second_group_filter[:, 1])
    length = grouped_head_inputs.shape[0]
    local_heads = head_decay_rate.shape[1]
    head_step_size = jax.nn.softplus(unsmoothed_step)
    decay_logarithm = extra_log_decay - head_step_size * head_decay_rate[None]
    values = conv_heads.reshape(length, 2, local_heads, HEAD) * head_step_size[:, :, :, None]
    state_one, local_one = scan_group(values[:, 0], decay_logarithm[:, 0], keys_one, queries_one)
    state_two, local_two = scan_group(values[:, 1], decay_logarithm[:, 1], keys_two, queries_two)
    running = jnp.cumsum(decay_logarithm, axis=0)
    device_log = running[-1]
    gathered = tuple(
        (
            part.astype(jnp.float32)
            for part in sent_together(
                (
                    device_log[None].astype(jnp.bfloat16),
                    state_one[None].astype(jnp.bfloat16),
                    state_two[None].astype(jnp.bfloat16),
                ),
                "sp",
                0,
                2,
            )
        )
    )
    logs_all = gathered[0]
    inclusive = jnp.cumsum(logs_all, axis=0)
    exclusive = inclusive - logs_all
    position = lax.axis_index("sp")
    device_ids = jnp.arange(lax.axis_size("sp"), dtype=jnp.int32)
    mine = jnp.sum(jnp.where((device_ids == position)[:, None, None], exclusive, 0.0), axis=0)
    earlier = (device_ids < position)[:, None, None]
    factors = jnp.exp(jnp.where(earlier, mine[None] - inclusive, -jnp.inf))
    enter_one = jnp.einsum("kh,khps->hps", factors[:, 0], gathered[1])
    enter_two = jnp.einsum("kh,khps->hps", factors[:, 1], gathered[2])
    carried_one = (
        jnp.einsum("ls,hps->lhp", queries_one, enter_one) * jnp.exp(running[:, 0])[:, :, None]
    )
    carried_two = (
        jnp.einsum("ls,hps->lhp", queries_two, enter_two) * jnp.exp(running[:, 1])[:, :, None]
    )
    mixer = jnp.stack([local_one + carried_one, local_two + carried_two], axis=1)
    gated = mixer * jax.nn.silu(head_gate_inputs.astype(jnp.float32)).reshape(
        length, 2, local_heads, HEAD
    )
    scaled = gated * lax.rsqrt(jnp.mean(gated * gated, axis=3, keepdims=True) + EPSILON)
    mixed = (scaled.reshape(length, 2, -1) * head_norm_gain[None]).astype(jnp.bfloat16)
    projected = jnp.einsum(
        "tgc,gcd->td",
        lax.all_gather(mixed, "tp", axis=2, tiled=True),
        output_weight,
        preferred_element_type=jnp.float32,
    )
    stream = (residual.astype(jnp.float32) + projected).astype(jnp.bfloat16)
    full_rows = lax.all_gather(stream, "tp", axis=1, tiled=True).astype(jnp.float32)
    normed = (
        full_rows
        * lax.rsqrt(jnp.mean(full_rows * full_rows, axis=1, keepdims=True) + EPSILON)
        * channel_norm_gain[None]
    ).astype(jnp.bfloat16)
    contract_last = (((1,), (1,)), ((), ()))
    pieces = side_by_side((channel_gate_weight, channel_up_weight), "sp", 0, 1)
    gate = jnp.dot(normed, pieces[0], preferred_element_type=jnp.float32)
    upward = jnp.dot(normed, pieces[1], preferred_element_type=jnp.float32)
    hidden = (jax.nn.silu(gate) * upward).astype(jnp.bfloat16)
    down_full = collect(channel_down_weight, "sp", 0)
    summed_rows = lax.psum_scatter(
        lax.dot_general(
            down_full, hidden, contract_last, preferred_element_type=jnp.float32
        ).astype(jnp.bfloat16),
        "tp",
        scatter_dimension=0,
        tiled=True,
    ).astype(jnp.float32)
    summed = summed_rows.T
    return (stream.astype(jnp.float32) + 0.5 * summed).astype(jnp.bfloat16)


def solution(mesh):
    return jax.shard_map(
        shards,
        mesh=mesh,
        in_specs=(
            P("sp", None, "tp"),
            P("sp", None, "tp"),
            P("sp", None, "tp"),
            P(None, "tp"),
            P("sp", None, "tp"),
            P("sp", None),
            P("sp", None),
            P("sp", None),
            P("sp", None),
            P(None, None, "tp"),
            P(),
            P(),
            P(None, "tp"),
            P(None, None, "tp"),
            P("sp", "tp"),
            P(),
            P("sp", "tp"),
            P("sp", "tp"),
            P("sp", "tp"),
        ),
        out_specs=P("sp", "tp"),
        check_vma=False,
    )
```

profile of v0, /device:TPU:1, one launch (start us, length us, event | category | flops | bytes accessed | tf_op | source)
XLA Modules:
  0.0 506.3 jit_solution(14219026784949340316)
XLA Ops:
  6.5 1.4 slice.232
  7.9 4.6 collective-permute-start.2
  13.8 3.2 collective-permute-start.1
  18.2 2.9 collective-permute-start
  21.2 1.4 slice.253
  22.5 3.2 collective-permute-start.4
  25.8 1.4 slice.245
  27.2 3.2 collective-permute-start.3
  31.3 1.7 convert_element_type.89
  33.0 1.8 convert_element_type.84
  34.8 1.8 convert_element_type.86
  37.7 1.4 slice_bitcast_fusion.17
  39.1 1.4 slice_bitcast_fusion.9
  41.8 1.4 multiply_subtract_fusion
  50.6 1.6 multiply_bitcast_fusion
  54.4 2.8 divide_multiply_fusion.2
  57.8 2.2 divide_multiply_fusion.1
  60.7 2.3 divide_multiply_fusion
  63.0 1.6 copy.86
  66.6 44.3 %while.27 = (s32[]{:T(128)}, f32[2,64,64]{2,1,0:T(8,128)S(1)}, f32[8,128,2,64]{1,0,3,2:T(8,128)S(1)}, f32[8,128,2]{2,1,0:T(8,128)}, f32[8,128,2,64]{1,0,3,2:T(8,...) while((s32[]{:T(128)}, f32[2,64,64]{2,1,0:T(8,128)S(1)}, ...), condition=%wide.region_7.8_spmd.clone, body=%wide.region_5.7_spmd.clone.sunk | while | flops 10715139 | bytes 1130684 | solution.py:95
  112.0 59.4 %while.26 = (s32[]{:T(128)}, f32[2,64,128]{2,1,0:T(8,128)S(1)}, f32[8,128,2,64]{1,0,3,2:T(8,128)}, f32[8,128,2]{2,1,0:T(8,128)}, f32[8,128,2,64]{1,0,3,2:T(8,128...) while((s32[]{:T(128)}, f32[2,64,128]{2,1,0:T(8,128)S(1)}, ...), condition=%wide.region_2.3_spmd.clone, body=%wide.region_0.2_spmd.clone.sunk | while | flops 17039364 | bytes 1098944 | solution.py:95
  116.7 2.8 dynamic_update_slice.11
  124.1 2.8 dynamic_update_slice.11
  131.5 2.8 dynamic_update_slice.11
  138.9 2.8 dynamic_update_slice.11
  146.3 2.8 dynamic_update_slice.11
  153.8 2.8 dynamic_update_slice.11
  161.2 2.8 dynamic_update_slice.11
  168.6 2.8 dynamic_update_slice.11
  172.7 2.1 slice_exponential_fusion.1
  178.8 1.9 reshape.225
  180.7 1.9 reshape.217
  182.7 65.0 %all-gather.5.cloned.1.call-done = bf16[32,2,12290]{2,1,0:T(2,128)(2,1)} async-done(((bf16[1,2,12290]{2,1,0:T(2,128)(2,1)}), bf16[32,2,12290]{2,1,0:T(2,128)(2,1)}) %all-gather.5.cloned.1.call-update) | async-done | bytes 1573136 | tf_op jit(solution)/shard_map/all_gather | solution.py:23
  248.9 2.7 slice.303
  255.4 1.8 slice.306
  258.6 1.7 fusion.61
  262.0 2.5 fusion.82
  264.7 40.4 %all-gather.7.cloned.1.call-done = bf16[1024,2,1024]{2,0,1:T(8,128)(2,1)} async-done(((bf16[1024,2,128]{2,0,1:T(8,128)(2,1)}), bf16[1024,2,1024]{2,0,1:T(8,128)(2,1)}) %all-gather.7.cloned.1.call-update) | async-done | bytes 4194320 | tf_op jit(solution)/shard_map/all_gather | solution.py:185
  305.1 4.3 fusion.60
  310.2 1.8 broadcast_in_dim.93
  312.1 9.8 %all-to-all-start = ((bf16[32,64,640]{2,1,0:T(8,128)(2,1)}), bf16[32,64,640]{2,1,0:T(8,128)(2,1)}, u32[]{:S(2)}, u32[]{:S(2)}) async-start(bf16[32,64,640]{2,1,0:T(8,128)(2,1)} %broadcast_in_dim.93), calls=%async_computation | async-start | bytes 5242880 | tf_op jit(solution)/shard_map/all_to_all | solution.py:48
  322.2 26.5 %all-gather.9.cloned.1.call-done = bf16[1024,2048]{1,0:T(8,128)(2,1)} async-done(((bf16[1024,256]{1,0:T(8,128)(2,1)}), bf16[1024,2048]{1,0:T(8,128)(2,1)}) %all-gather.9.cloned.1.call-update) | async-done | bytes 4194320 | tf_op jit(solution)/shard_map/all_gather | solution.py:190
  348.6 3.1 fusion.50
  351.7 86.9 %all-gather.11.cloned.1.call-done = bf16[2048,1280]{1,0:T(8,128)(2,1)} async-done(((bf16[64,1280]{1,0:T(8,128)(2,1)}), bf16[2048,1280]{1,0:T(8,128)(2,1)}) %all-gather.11.cloned.1.call-update) | async-done | bytes 5242896 | tf_op jit(solution)/shard_map/all_gather | solution.py:33
  438.6 8.0 %fusion.53 = f32[1024,640]{1,0:T(8,128)} fusion(bf16[2048,1280]{1,0:T(8,128)(2,1)} %all-gather.11.cloned.1.call-done, bf16[1024,2048]{1,0:T(8,128)(2,1)} %all-gather.9.cloned.1.call-done, f32[2048]{0:T(1024)S(1)} %copy-done.15, f32[1024]{0:T(1024)S(1)} %add_rsqrt_fusion.1), kind=kOutput, calls=%fused_computation.74 | convolution fusion | flops 2692743168 | bytes 9449472 | tf_op jit(solution)/shard_map/dot_general | solution.py:199
  446.5 13.2 %convert_bitcast_fusion = bf16[2048,1024]{0,1:T(8,128)(2,1)} fusion(bf16[2048,640]{1,0:T(8,128)(2,1)} %bitcast.50, f32[1024,640]{1,0:T(8,128)} %fusion.53, bf16[2048,1280]{1,0:T(8,128)(2,1)} %all-gather.11.cloned.1.call-done, bf16[1024,2048]{1,0:T(8,128)(2,1)} %all-gather.9.cloned.1.call-done, f32[2048]{0:T(1024)S(1)} %copy-done.15, ...), kind=kOutput, calls=%fused_computation.73 | convolution fusion | flops 5383127040 | bytes 16265216 | tf_op jit(solution)/shard_map/dot_general | solution.py:203
  459.8 38.0 %reduce-scatter.2.cloned.1.call-done = bf16[256,1024]{0,1:T(8,128)(2,1)} async-done(((bf16[2048,1024]{0,1:T(8,128)(2,1)}), bf16[256,1024]{0,1:T(8,128)(2,1)}) %reduce-scatter.2.cloned.1.call-update) | async-done | bytes 524304 | tf_op jit(solution)/shard_map/reduce_scatter | solution.py:202
  497.8 2.0 fusion.85
  (349 shorter events, 115.0 us)
Async XLA Ops:
  6.5 298.5 %copy-start = (bf16[2,1024,256]{2,1,0:T(8,128)(2,1)S(1)}, bf16[2,1024,256]{2,1,0:T(8,128)(2,1)}, u32[]{:S(2)}) copy-start(bf16[2,1024,256]{2,1,0:T(8,128)(2,1)} %param.36) | copy-start | bytes 3145732
  6.5 241.2 %all-gather.5.cloned.1.call-start = ((), (), s32[]{:S(2)}) async-start(), calls=%async_computation.2 | async-start | bytes 1638912 | tf_op jit(solution)/shard_map/all_gather | solution.py:23
  7.9 49.2 %collective-permute-start.2 = (bf16[3,128]{1,0:T(4,128)(2,1)}, bf16[3,128]{1,0:T(4,128)(2,1)}, u32[]{:S(2)}, u32[]{:S(2)}) collective-permute-start(bf16[3,128]{1,0:T(4,128)(2,1)} %slice.232), channel_id=1, source_target_pairs={{0,8},{8,16},{16,24},{24,32},{32,40},{40,48},{48,56},{56,64},{64,7... | collective-permute-start | bytes 2312 | tf_op jit(solution)/shard_map/ppermute | solution.py:17
  13.8 39.9 %collective-permute-start.1 = (bf16[3,128]{1,0:T(4,128)(2,1)}, bf16[3,128]{1,0:T(4,128)(2,1)}, u32[]{:S(2)}, u32[]{:S(2)}) collective-permute-start(bf16[3,128]{1,0:T(4,128)(2,1)} %slice.224), channel_id=1, source_target_pairs={{0,8},{8,16},{16,24},{24,32},{32,40},{40,48},{48,56},{56,64},{64,7... | collective-permute-start | bytes 2312 | tf_op jit(solution)/shard_map/ppermute | solution.py:17
  18.2 41.8 %collective-permute-start = (bf16[3,2,128]{2,0,1:T(4,128)(2,1)}, bf16[3,2,128]{2,0,1:T(4,128)(2,1)}, u32[]{:S(2)}, u32[]{:S(2)}) collective-permute-start(bf16[3,2,128]{2,0,1:T(4,128)(2,1)} %copy.138), channel_id=1, source_target_pairs={{0,8},{8,16},{16,24},{24,32},{32,40},{40,48},{48,56},{56,64},{64,7... | collective-permute-start | bytes 4616 | tf_op jit(solution)/shard_map/ppermute | solution.py:17
  22.5 25.6 %collective-permute-start.4 = (bf16[3,64]{0,1:T(8,128)(2,1)}, bf16[3,64]{0,1:T(8,128)(2,1)}, u32[]{:S(2)}, u32[]{:S(2)}) collective-permute-start(bf16[3,64]{0,1:T(8,128)(2,1)} %slice.253), channel_id=1, source_target_pairs={{0,8},{8,16},{16,24},{24,32},{32,40},{40,48},{48,56},{56,64},{64,7... | collective-permute-start | bytes 1160 | tf_op jit(solution)/shard_map/ppermute | solution.py:17
  27.2 22.7 %collective-permute-start.3 = (bf16[3,64]{0,1:T(8,128)(2,1)}, bf16[3,64]{0,1:T(8,128)(2,1)}, u32[]{:S(2)}, u32[]{:S(2)}) collective-permute-start(bf16[3,64]{0,1:T(8,128)(2,1)} %slice.245), channel_id=1, source_target_pairs={{0,8},{8,16},{16,24},{24,32},{32,40},{40,48},{48,56},{56,64},{64,7... | collective-permute-start | bytes 1160 | tf_op jit(solution)/shard_map/ppermute | solution.py:17
  31.3 25.9 %copy-start.5 = (f32[1024,64]{0,1:T(8,128)}, f32[1024,64]{0,1:T(8,128)S(1)}, u32[]{:S(2)}) copy-start(f32[1024,64]{0,1:T(8,128)S(1)} %convert_element_type.91) | copy-start | bytes 786436
  47.5 17.1 %copy-start.11 = (f32[1024,2,2]{0,2,1:T(2,128)S(1)}, f32[1024,2,2]{0,2,1:T(2,128)}, u32[]{:S(2)}) copy-start(f32[1024,2,2]{0,2,1:T(2,128)} %get-tuple-element.190) | copy-start | bytes 49156
  48.8 1.8 copy-start.7
  111.0 1.0 copy-start.4
  112.0 59.6 %copy-start.14 = (bf16[1,2,2]{2,1,0:T(2,128)(2,1)S(1)}, bf16[1,2,2]{2,1,0:T(2,128)(2,1)}, u32[]{:S(2)}) copy-start(bf16[1,2,2]{2,1,0:T(2,128)(2,1)} %slice.501) | copy-start | bytes 28
  112.0 65.2 %copy-start.3 = (bf16[1024,2,128]{2,1,0:T(2,128)(2,1)S(1)}, bf16[1024,2,128]{2,1,0:T(2,128)(2,1)}, u32[]{:S(2)}) copy-start(bf16[1024,2,128]{2,1,0:T(2,128)(2,1)} %param.24) | copy-start | bytes 1572868
  172.4 132.6 %all-gather.7.cloned.1.call-start = ((), (), s32[]{:S(2)}) async-start(), calls=%async_computation.3 | async-start | bytes 4718592 | tf_op jit(solution)/shard_map/all_gather | solution.py:185
  251.6 7.0 %copy-start.12 = (f32[64]{0:T(128)S(1)}, f32[64]{0:T(128)}, u32[]{:S(2)}) copy-start(f32[64]{0:T(128)} %get-tuple-element.213) | copy-start | bytes 772
  254.4 4.2 copy-start.6
  258.6 2.7 copy-start.1
  258.6 3.4 copy-start.13
  264.6 44.9 %copy-start.8 = (bf16[64,640]{1,0:T(8,128)(2,1)S(1)}, bf16[64,640]{1,0:T(8,128)(2,1)}, u32[]{:S(2)}) copy-start(bf16[64,640]{1,0:T(8,128)(2,1)} %param.40) | copy-start | bytes 245764
  264.6 44.9 %copy-start.9 = (bf16[64,640]{1,0:T(8,128)(2,1)S(1)}, bf16[64,640]{1,0:T(8,128)(2,1)}, u32[]{:S(2)}) copy-start(bf16[64,640]{1,0:T(8,128)(2,1)} %param.39) | copy-start | bytes 245764
  264.6 45.6 %copy-start.10 = (bf16[64,640]{1,0:T(8,128)(2,1)S(1)}, bf16[64,640]{1,0:T(8,128)(2,1)}, u32[]{:S(2)}) copy-start(bf16[64,640]{1,0:T(8,128)(2,1)} %param.41) | copy-start | bytes 245764
  264.6 84.0 %all-gather.9.cloned.1.call-start = ((), (), s32[]{:S(2)}) async-start(), calls=%async_computation.4 | async-start | bytes 4718592 | tf_op jit(solution)/shard_map/all_gather | solution.py:190
  309.4 129.1 %all-gather.11.cloned.1.call-start = ((), (), s32[]{:S(2)}) async-start(), calls=%async_computation.5 | async-start | bytes 5406720 | tf_op jit(solution)/shard_map/all_gather | solution.py:33
  312.1 126.5 %copy-start.15 = (f32[2048]{0:T(1024)S(1)}, f32[2048]{0:T(1024)}, u32[]{:S(2)}) copy-start(f32[2048]{0:T(1024)} %param.38) | copy-start | bytes 24580
  312.1 134.5 %all-to-all-start = ((bf16[32,64,640]{2,1,0:T(8,128)(2,1)}), bf16[32,64,640]{2,1,0:T(8,128)(2,1)}, u32[]{:S(2)}, u32[]{:S(2)}) async-start(bf16[32,64,640]{2,1,0:T(8,128)(2,1)} %broadcast_in_dim.93), calls=%async_computation | async-start | bytes 5242880 | tf_op jit(solution)/shard_map/all_to_all | solution.py:48
  321.9 175.9 %reduce-scatter.2.cloned.1.call-start = ((), (), s32[]{:S(2)}) async-start(), calls=%async_computation.6 | async-start | bytes 4718592 | tf_op jit(solution)/shard_map/reduce_scatter | solution.py:202
  459.7 38.1 %copy-start.2 = (bf16[1024,256]{1,0:T(8,128)(2,1)S(1)}, bf16[1024,256]{1,0:T(8,128)(2,1)}, u32[]{:S(2)}) copy-start(bf16[1024,256]{1,0:T(8,128)(2,1)} %fusion.60) | copy-start | bytes 1572868
Sparse Core Ops, SparseCore 0:
  172.5 75.1 all-gather.4
  264.7 40.3 all-gather.6
  309.6 39.0 all-gather.8
  351.1 87.4 all-gather.10
  459.9 37.8 reduce-scatter.1
where the time goes:
time: 513 us; the launch traced here: 506 us
  waiting for transfers between devices  257 us (50%)
  local copies, waits for them, and re-layouts  117 us (23%)
  matrix products  53.2 us (10%)
  other arithmetic  37.3 us (7%)
  starting transfers between devices  27.5 us (5%)
  between operations  13.5 us (3%)
    all_gather x1, waiting for transfers between devices, side_by_side(): out, at, done = (lax.all_gather(both, axis, axis=dim, tiled=True), 0, [])  86.9 us
    all_gather x1, waiting for transfers between devices, sent_together(): out, at, done = (lax.all_gather(both, axis, axis=dim, tiled=True), 0, [])  65 us
    all_gather x1, waiting for transfers between devices, shards(): lax.all_gather(mixed, 'tp', axis=2, tiled=True)  40.4 us
    reduce_scatter x1, waiting for transfers between devices, shards(): lax.psum_scatter(lax.dot_general(down_full, hidden, contract_last, prefer...  38 us
    dynamic_update_slice x16, local copies, waits for them, and re-layouts, scan_group(): final_state, outputs = lax.scan(advance, initial, blocks)  32.7 us
    all_gather x1, waiting for transfers between devices, shards(): lax.all_gather(stream, 'tp', axis=1, tiled=True).astype(jnp.float32)  26.5 us
    dynamic_slice x24, local copies, waits for them, and re-layouts, scan_group(): final_state, outputs = lax.scan(advance, initial, blocks)  26.4 us
    ppermute x5, starting transfers between devices, from_behind(): return lax.ppermute(block, axis, route)  17.1 us
  transfers between devices with their start and end apart: 11, of which 5 were waited for; matrix products, arithmetic and copies ran while one was open for 12% of the time, Pallas kernels for 0%

commit v1 on v0

v1 whole, which is shorter than its diff:
```python
import functools

import jax
import jax.numpy as jnp
from jax import lax
from jax.experimental import pallas as pl
from jax.experimental.pallas import tpu as pltpu
from jax.sharding import PartitionSpec as P

HEAD = 64
CONV = 4
BLOCK = 128
EPSILON = 1e-06
MESH = pl.DeviceIdType.MESH
F32 = jnp.float32
BF16 = jnp.bfloat16
NY = 4
NZ = 8
QROWS = 48
MROWS = 64


def silu(v):
    return v * (1.0 / (1.0 + jnp.exp(-v)))


def halves(lane_low, a, b):
    return jnp.where(lane_low, a, b)


def dot(a, b, ca, cb):
    return lax.dot_general(a, b, (((ca,), (cb,)), ((), ())), preferred_element_type=F32)


def split_three(v):
    hi = v.astype(BF16)
    rest = v - hi.astype(F32)
    mid = rest.astype(BF16)
    low = (rest - mid.astype(F32)).astype(BF16)
    return hi.astype(F32), mid.astype(F32), low.astype(F32)


def log_rows(l0, l1):
    rows = []
    for part0, part1 in zip(split_three(l0), split_three(l1)):
        rows += [part0, part1]
    rows.append(jnp.zeros((10, 128), F32))
    return jnp.concatenate(rows, axis=0).astype(BF16)


def read_logs(rows):
    v = rows.astype(F32)
    return v[0:1] + v[2:3] + v[4:5], v[1:2] + v[3:4] + v[5:6]


def front_kernel(
    xs, gs, k1, q1, kq2, table, head_taps, taps1, taps2, gain,
    mixed,
    rim, keys, queries, values, local, cols, erun, state, starts,
    msg1, buf1, msg2, buf2, msg3, enter,
    rim_send, rim_recv, send1, recv1, send2, recv2, send3, recv3,
):
    sp = lax.axis_index("sp")
    y = lax.rem(sp, NY)
    z = sp // NY
    n_sp = NY * NZ
    blocks = xs.shape[1] // BLOCK
    right = lax.rem(sp + 1, n_sp)
    left = lax.rem(sp + n_sp - 1, n_sp)
    y_peers = [z * NY + lax.rem(y + j, NY) for j in range(1, NY)]
    z_peers = [lax.rem(z + j, NZ) * NY + y for j in range(1, NZ)]

    barrier = pltpu.get_barrier_semaphore()
    for peer in [right, left] + y_peers + z_peers:
        pl.semaphore_signal(barrier, inc=1, device_id={"sp": peer}, device_id_type=MESH)
    pl.semaphore_wait(barrier, 2 + (NY - 1) + (NZ - 1))

    tail = pl.ds(xs.shape[1] - 16, 16)
    rim_copies = []
    for n, src in enumerate([xs.at[0, tail], xs.at[1, tail], k1.at[tail], q1.at[tail], kq2.at[tail]]):
        copy = pltpu.make_async_remote_copy(
            src_ref=src, dst_ref=rim.at[n], send_sem=rim_send.at[n], recv_sem=rim_recv.at[n],
            device_id={"sp": right}, device_id_type=MESH)
        copy.start()
        rim_copies.append(copy)

    lane = lax.broadcasted_iota(jnp.int32, (8, 128), 1)
    row8 = lax.broadcasted_iota(jnp.int32, (8, 128), 0)
    low = lax.broadcasted_iota(jnp.int32, (BLOCK, 128), 1) < HEAD
    low1 = lax.broadcasted_iota(jnp.int32, (1, 128), 1) < HEAD
    causal = lax.broadcasted_iota(jnp.int32, (BLOCK, BLOCK), 0) >= lax.broadcasted_iota(
        jnp.int32, (BLOCK, BLOCK), 1)

    state[...] = jnp.zeros_like(state)
    for copy in rim_copies:
        copy.wait()
    has_left = sp > 0
    tails = tuple(
        jnp.where(has_left, rim[n].astype(F32)[8:16], 0.0) for n in range(5))

    def conv(block, before, taps):
        full = jnp.concatenate([before, block], axis=0)
        total = taps[0] * full[5 : 5 + BLOCK]
        for k in range(1, CONV):
            total = total + taps[k] * full[5 + k : 5 + k + BLOCK]
        return silu(total)

    def first(b, carry):
        before, offs = carry[:5], carry[5]
        at = pl.ds(pl.multiple_of(b * BLOCK, BLOCK), BLOCK)
        r = table[b]
        c = r
        for s in (1, 2, 4, 8, 16, 32, 64):
            c = c + jnp.where(lane >= s, pltpu.roll(c, s, 1), 0.0)
        t = jnp.where(row8 < 4, c, r).T
        cols[b] = t
        erun[b] = jnp.exp(jnp.where(row8 < 4, c + offs, 0.0)).T
        raw = [xs[0, at].astype(F32), xs[1, at].astype(F32), k1[at].astype(F32),
               q1[at].astype(F32), kq2[at].astype(F32)]
        key_one = conv(raw[2], before[2], [taps1[k, 0:1] for k in range(CONV)])
        query_one = conv(raw[3], before[3], [taps1[k, 1:2] for k in range(CONV)])
        both = conv(raw[4], before[4], [taps2[k : k + 1] for k in range(CONV)])
        key_two = jnp.where(low, both, 0.0)
        query_two = jnp.where(low, pltpu.roll(both, 64, 1), 0.0)
        for g, (key, query) in enumerate([(key_one, query_one), (key_two, query_two)]):
            u = conv(raw[g], before[g], [head_taps[k, g : g + 1] for k in range(CONV)])
            h = 2 * g
            v = u * halves(low, t[:, 4 + h : 5 + h], t[:, 5 + h : 6 + h])
            cum = halves(low, t[:, h : h + 1], t[:, h + 1 : h + 2])
            total = halves(low1, c[h : h + 1, 127:128], c[h + 1 : h + 2, 127:128])
            to_end = jnp.exp(total - cum)
            kb = key.astype(BF16)
            keys[g, at] = kb
            queries[g, at] = query.astype(BF16)
            values[g, at] = v.astype(BF16)
            old = state[g]
            starts[g, b] = old.astype(BF16)
            state[g] = old * jnp.exp(total) + dot(kb, (v * to_end).astype(BF16), 0, 0)
        offs = offs + jnp.broadcast_to(c[:, 127:128], (8, 128))
        return tuple(v[BLOCK - 8 :] for v in raw) + (offs,)

    carry = lax.fori_loop(0, blocks, first, tails + (jnp.zeros((8, 128), F32),))
    offs = carry[5]
    log0 = halves(low1, offs[0:1], offs[1:2])
    log1 = halves(low1, offs[2:3], offs[3:4])

    logs = log_rows(log0, log1)
    full_state = jnp.concatenate([state[0], state[1][0:64]], axis=0).astype(BF16)
    for q in range(NY):
        msg1[q, 0:QROWS] = full_state[q * QROWS : (q + 1) * QROWS]
        msg1[q, QROWS:MROWS] = logs
    copies1 = []
    for j in range(1, NY):
        to = lax.rem(y + j, NY)
        copy = pltpu.make_async_remote_copy(
            src_ref=msg1.at[to], dst_ref=buf1.at[y], send_sem=send1.at[j - 1],
            recv_sem=recv1.at[j - 1], device_id={"sp": z * NY + to}, device_id_type=MESH)
        copy.start()
        copies1.append(copy)
    buf1[y] = msg1[y]

    def inside(b, carry):
        at = pl.ds(pl.multiple_of(b * BLOCK, BLOCK), BLOCK)
        t = cols[b]
        crow = t.T
        for g in range(2):
            h = 2 * g
            qb, kb, v = queries[g, at], keys[g, at], values[g, at]
            scores = dot(qb, kb, 1, 1)
            weights = []
            for j in range(2):
                span = t[:, h + j : h + j + 1] - crow[h + j : h + j + 1]
                weights.append((jnp.exp(jnp.where(causal, span, -jnp.inf)) * scores).astype(BF16))
            zero = jnp.zeros_like(v)
            two = jnp.concatenate([jnp.where(low, v, zero), jnp.where(low, zero, v)], axis=0)
            out = dot(jnp.concatenate(weights, axis=1), two, 1, 0)
            cum = halves(low, t[:, h : h + 1], t[:, h + 1 : h + 2])
            local[g, at] = out + dot(qb, starts[g, b], 1, 0) * jnp.exp(cum)
        return carry

    lax.fori_loop(0, blocks // 2, inside, 0)

    for copy in copies1:
        copy.wait()
    rows = y * QROWS + lax.broadcasted_iota(jnp.int32, (QROWS, 128), 0)
    group_one = rows < 128

    def factor(f0, f1):
        return jnp.where(group_one, f0, f1)

    prefix, befores = [], []
    run = jnp.zeros((QROWS, 128), F32)
    sum0 = jnp.zeros((1, 128), F32)
    sum1 = jnp.zeros((1, 128), F32)
    for j in range(NY):
        prefix.append(run)
        befores.append((sum0, sum1))
        l0, l1 = read_logs(buf1[j, QROWS:MROWS])
        run = run * factor(jnp.exp(l0), jnp.exp(l1)) + buf1[j, 0:QROWS].astype(F32)
        sum0, sum1 = sum0 + l0, sum1 + l1
    msg2[0:QROWS] = run.astype(BF16)
    msg2[QROWS:MROWS] = log_rows(sum0, sum1)
    copies2 = []
    for j in range(1, NZ):
        copy = pltpu.make_async_remote_copy(
            src_ref=msg2, dst_ref=buf2.at[z], send_sem=send2.at[j - 1],
            recv_sem=recv2.at[j - 1], device_id={"sp": lax.rem(z + j, NZ) * NY + y},
            device_id_type=MESH)
        copy.start()
        copies2.append(copy)
    buf2[z] = msg2[...]

    lax.fori_loop(blocks // 2, blocks, inside, 0)

    for copy in copies2:
        copy.wait()
    run = jnp.zeros((QROWS, 128), F32)
    for j in range(NZ):
        l0, l1 = read_logs(buf2[j, QROWS:MROWS])
        new = run * factor(jnp.exp(l0), jnp.exp(l1)) + buf2[j, 0:QROWS].astype(F32)
        run = jnp.where(j < z, new, run)
    for j in range(NY):
        l0, l1 = befores[j]
        msg3[j] = (run * factor(jnp.exp(l0), jnp.exp(l1)) + prefix[j]).astype(BF16)
    mine = pl.ds(pl.multiple_of(y * QROWS, 16), QROWS)
    copies3 = []
    for j in range(1, NY):
        to = lax.rem(y + j, NY)
        copy = pltpu.make_async_remote_copy(
            src_ref=msg3.at[to], dst_ref=enter.at[mine], send_sem=send3.at[j - 1],
            recv_sem=recv3.at[j - 1], device_id={"sp": z * NY + to}, device_id_type=MESH)
        copy.start()
        copies3.append(copy)
    enter[mine] = msg3[y]
    for copy in copies3:
        copy.wait()

    enter_one = enter[0:128]
    enter_two = jnp.concatenate([enter[128:192], jnp.zeros((64, 128), BF16)], axis=0)

    def finish(b, carry):
        at = pl.ds(pl.multiple_of(b * BLOCK, BLOCK), BLOCK)
        e = erun[b]
        for g, entering in enumerate([enter_one, enter_two]):
            h = 2 * g
            m = local[g, at] + dot(queries[g, at], entering, 1, 0) * halves(
                low, e[:, h : h + 1], e[:, h + 1 : h + 2])
            m = m * silu(gs[g, at].astype(F32))
            square = m * m
            s0 = jnp.sum(jnp.where(low, square, 0.0), axis=1, keepdims=True)
            s1 = jnp.sum(jnp.where(low, 0.0, square), axis=1, keepdims=True)
            scale = lax.rsqrt(halves(low, s0, s1) * (1.0 / HEAD) + EPSILON)
            mixed[g, at] = (m * scale * gain[g : g + 1]).astype(BF16)
        return carry

    lax.fori_loop(0, blocks, finish, 0)


def front(xs, gs, k1, q1, kq2, table, head_taps, taps1, taps2, gain):
    length = xs.shape[1]
    blocks = length // BLOCK
    vmem = pl.BlockSpec(memory_space=pltpu.VMEM)
    dma = pltpu.SemaphoreType.DMA
    return pl.pallas_call(
        front_kernel,
        out_shape=jax.ShapeDtypeStruct((2, length, 128), BF16),
        in_specs=[vmem] * 10,
        out_specs=vmem,
        scratch_shapes=[
            pltpu.VMEM((5, 16, 128), BF16),
            pltpu.VMEM((2, length, 128), BF16),
            pltpu.VMEM((2, length, 128), BF16),
            pltpu.VMEM((2, length, 128), BF16),
            pltpu.VMEM((2, length, 128), F32),
            pltpu.VMEM((blocks, BLOCK, 8), F32),
            pltpu.VMEM((blocks, BLOCK, 8), F32),
            pltpu.VMEM((2, 128, 128), F32),
            pltpu.VMEM((2, blocks, 128, 128), BF16),
            pltpu.VMEM((NY, MROWS, 128), BF16),
            pltpu.VMEM((NY, MROWS, 128), BF16),
            pltpu.VMEM((MROWS, 128), BF16),
            pltpu.VMEM((NZ, MROWS, 128), BF16),
            pltpu.VMEM((NY, QROWS, 128), BF16),
            pltpu.VMEM((NY * QROWS, 128), BF16),
            dma((5,)), dma((5,)),
            dma((NY - 1,)), dma((NY - 1,)),
            dma((NZ - 1,)), dma((NZ - 1,)),
            dma((NY - 1,)), dma((NY - 1,)),
        ],
        compiler_params=pltpu.CompilerParams(
            collective_id=0, has_side_effects=True, vmem_limit_bytes=24 * 1024 * 1024),
        cost_estimate=pl.CostEstimate(
            flops=4_000_000_000, bytes_accessed=4_000_000, transcendentals=4_000_000),
        name="front",
    )(xs, gs, k1, q1, kq2, table, head_taps, taps1, taps2, gain)


def shards(
    grouped_head_inputs,
    head_gate_inputs,
    unsmoothed_step,
    head_decay_rate,
    extra_log_decay,
    first_group_keys,
    first_group_queries,
    second_group_keys,
    second_group_queries,
    head_input_filter,
    first_group_filter,
    second_group_filter,
    head_norm_gain,
    output_weight,
    residual,
    channel_norm_gain,
    channel_gate_weight,
    channel_up_weight,
    channel_down_weight,
):
    length = grouped_head_inputs.shape[0]
    blocks = length // BLOCK
    step = jax.nn.softplus(unsmoothed_step)
    log_decay = extra_log_decay - step * head_decay_rate[None]
    table = jnp.stack([log_decay, step]).reshape(2, blocks, BLOCK, 4)
    table = table.transpose(1, 0, 3, 2).reshape(blocks, 8, BLOCK)
    mixed = front(
        grouped_head_inputs.transpose(1, 0, 2),
        head_gate_inputs.transpose(1, 0, 2),
        first_group_keys,
        first_group_queries,
        jnp.concatenate([second_group_keys, second_group_queries], axis=1),
        table,
        head_input_filter,
        first_group_filter,
        second_group_filter.reshape(CONV, 128),
        head_norm_gain,
    )
    whole = lax.all_gather(mixed, "tp", axis=0)
    projected = lax.dot_general(
        whole,
        output_weight.reshape(2, 8, 128, output_weight.shape[2]),
        (((0, 1, 3), (1, 0, 2)), ((), ())),
        preferred_element_type=F32,
    )
    stream = (residual.astype(F32) + projected).astype(BF16)
    full_rows = lax.all_gather(stream, "tp", axis=1, tiled=True).astype(F32)
    normed = (
        full_rows
        * lax.rsqrt(jnp.mean(full_rows * full_rows, axis=1, keepdims=True) + EPSILON)
        * channel_norm_gain[None]
    ).astype(BF16)
    width = channel_gate_weight.shape[1]
    weights = lax.all_gather(
        jnp.concatenate([channel_gate_weight, channel_up_weight, channel_down_weight], axis=1),
        "sp", axis=0, tiled=True)
    gate = jnp.dot(normed, weights[:, :width], preferred_element_type=F32)
    upward = jnp.dot(normed, weights[:, width : 2 * width], preferred_element_type=F32)
    hidden = (jax.nn.silu(gate) * upward).astype(BF16)
    partial = dot(weights[:, 2 * width :], hidden, 1, 1).astype(BF16)
    summed = lax.psum_scatter(partial, "tp", scatter_dimension=0, tiled=True).astype(F32).T
    return (stream.astype(F32) + 0.5 * summed).astype(BF16)


def solution(mesh):
    return jax.shard_map(
        shards,
        mesh=mesh,
        in_specs=(
            P("sp", None, "tp"),
            P("sp", None, "tp"),
            P("sp", None, "tp"),
            P(None, "tp"),
            P("sp", None, "tp"),
            P("sp", None),
            P("sp", None),
            P("sp", None),
            P("sp", None),
            P(None, None, "tp"),
            P(),
            P(),
            P(None, "tp"),
            P(None, None, "tp"),
            P("sp", "tp"),
            P(),
            P("sp", "tp"),
            P("sp", "tp"),
            P("sp", "tp"),
        ),
        out_specs=P("sp", "tp"),
        check_vma=False,
    )
```

time: 513 us -> 294 us (0.57)
  local copies, waits for them, and re-layouts: 117 us -> 8.39 us
  waiting for transfers between devices: 257 us -> 202 us
  Pallas kernels: 0 us -> 35.2 us
  other arithmetic: 37.3 us -> 6.77 us
  matrix products: 53.2 us -> 25.4 us
  starting transfers between devices: 27.5 us -> 0.13 us
    all_gather x4 -> x3, waiting for transfers between devices: 219 us -> 167 us  [the longest x1 94.6 us: shards(): lax.all_gather(jnp.concatenate([channel_gate_weight, channel_up_weight, c...]
    pallas_call x0 -> x1, Pallas kernels: none -> 35.2 us  [front(): pl.pallas_call(front_kernel, out_shape=jax.ShapeDtypeStruct((2, length, 1...]
    dynamic_update_slice x16 -> x0, local copies, waits for them, and re-layouts: 32.7 us -> none  [scan_group(): final_state, outputs = lax.scan(advance, initial, blocks)]
    dot_general x71 -> x3, matrix products: 53.2 us -> 25.4 us  [the longest x1 13.1 us: dot(): lax.dot_general(a, b, (((ca,), (cb,)), ((), ())), preferred_element_type=...]
    dynamic_slice x24 -> x0, local copies, waits for them, and re-layouts: 26.4 us -> none  [scan_group(): final_state, outputs = lax.scan(advance, initial, blocks)]
    ppermute x5 -> x0, starting transfers between devices: 17.1 us -> none  [from_behind(): return lax.ppermute(block, axis, route)]
    squeeze x32 -> x0, local copies, waits for them, and re-layouts: 13.7 us -> none  [the longest x16 13.6 us: scan_group(): final_state, outputs = lax.scan(advance, initial, blocks)]
    slice x16 -> x0, local copies, waits for them, and re-layouts: 13.7 us -> none  [the longest x2 4.5 us: sent_together(): share = out[..., at:at + column.shape[along]]]
  transfers between devices with their start and end apart: 11 -> 4, of which waited for: 5 -> 4; matrix products, arithmetic and copies ran while one was open for 12% -> 1% of each run, Pallas kernels for 0% -> 0%
where the time goes in v1:
time: 294 us; the launch traced here: 292 us
  waiting for transfers between devices  202 us (69%)
  Pallas kernels  35.2 us (12%)
  matrix products  25.4 us (9%)
  between operations  13.3 us (5%)
  local copies, waits for them, and re-layouts  8.39 us (3%)
  other arithmetic  6.77 us (2%)
    all_gather x1, waiting for transfers between devices, shards(): lax.all_gather(jnp.concatenate([channel_gate_weight, channel_up_weight, c...  94.6 us
    all_gather x1, waiting for transfers between devices, shards(): full_rows = lax.all_gather(stream, 'tp', axis=1, tiled=True).astype(F32)  37.3 us
    reduce_scatter x1, waiting for transfers between devices, shards(): lax.psum_scatter(partial, 'tp', scatter_dimension=0, tiled=True).astype(F32)  35.6 us
    pallas_call x1, Pallas kernels, front(): pl.pallas_call(front_kernel, out_shape=jax.ShapeDtypeStruct((2, length, 1...  35.2 us
    all_gather x1, waiting for transfers between devices, shards(): whole = lax.all_gather(mixed, 'tp', axis=0)  34.7 us
    dot_general x1, matrix products, dot(): lax.dot_general(a, b, (((ca,), (cb,)), ((), ())), preferred_element_type=...  13.1 us
    dot_general x1, matrix products, shards(): jnp.dot(normed, weights[:, width:2 * width], preferred_element_type=F32)  7.98 us
    unnamed x26, local copies, waits for them, and re-layouts  6.15 us
  transfers between devices with their start and end apart: 4, of which 4 were waited for; matrix products, arithmetic and copies ran while one was open for 1% of the time, Pallas kernels for 0%

profile of v1, /device:TPU:1, one launch (start us, length us, event | category | flops | bytes accessed | tf_op | source)
XLA Modules:
  0.0 291.5 jit_solution(7537925543462031893)
XLA Ops:
  6.5 0.0 copy-start
  6.5 0.0 all-gather.9.cloned.1.call-start
  6.5 0.9 reshape.25.taps2
  7.4 0.8 multiply_subtract_fusion
  8.3 1.1 copy.30
  9.4 1.1 copy.31
  10.5 0.1 pad_maximum_fusion.kq2
  10.7 1.3 copy_bitcast_fusion
  12.0 0.0 copy-start.1
  12.0 0.9 copy-done.1
  13.0 0.0 copy-start.2
  13.0 0.9 copy-done.2
  13.9 0.7 copy-done.3
  14.6 0.0 copy-start.4
  14.6 0.7 copy-done.4
  15.3 0.0 copy-start.5
  15.3 0.7 copy-done.5
  16.0 0.0 copy-start.10
  16.0 35.2 %front.1 = bf16[2,1024,128]{2,1,0:T(8,128)(2,1)} custom-call(bf16[2,1024,128]{2,1,0:T(8,128)(2,1)S(1)} %get-tuple-element.8.xs, bf16[2,1024,128]{2,1,0:T(8,128)(2,1)S(1)} %get-tuple-element.7.gs, bf16[1024,128]{1,0:T(8,128)(2,1)S(1)} %copy-done.1, bf16[1024,128]{1,0:T(8,128)(2,1)S(1)} %copy-done.2, bf16[1024,128]{1,0:T(8,128)(2,1)S(1)} %pad_maximum_fusion.kq2, ...), custom_call_target="tpu_custom_call" | custom-call | flops 4000000000 | bytes 4000000 | tf_op jit(solution)/shard_map/front/pallas_call | solution.py:264
  51.2 0.0 all-gather.9.cloned.1.call-update
  51.2 0.0 all-gather.7.cloned.1.call-start
  51.3 34.7 %all-gather.9.cloned.1.call-done = bf16[16,1024,128]{2,1,0:T(8,128)(2,1)} async-done(((bf16[2,1024,128]{2,1,0:T(8,128)(2,1)}), bf16[16,1024,128]{2,1,0:T(8,128)(2,1)}) %all-gather.9.cloned.1.call-update) | async-done | bytes 4194320 | tf_op jit(solution)/shard_map/all_gather | solution.py:337
  86.0 0.0 copy-done
  86.0 0.0 copy-done.10
  86.0 0.0 copy-start.7
  86.0 0.0 copy-start.8
  86.0 0.0 copy-start.9
  86.0 4.3 %fusion.11 = bf16[1024,256]{1,0:T(8,128)(2,1)} fusion(bf16[8,2,1024,128]{3,2,1,0:T(8,128)(2,1)} %bitcast.28, bf16[2,8,128,256]{3,2,1,0:T(8,128)(2,1)S(1)} %bitcast.26, bf16[1024,256]{1,0:T(8,128)(2,1)S(1)} %copy-done.10), kind=kOutput, calls=%fused_computation.14 | convolution fusion | flops 1074528256 | bytes 6291456 | tf_op jit(solution)/shard_map/dot_general | solution.py:338
  90.3 0.0 copy-start.11
  90.3 0.0 all-gather.7.cloned.1.call-update
  90.3 0.0 all-gather.5.cloned.1.call-start
  90.4 0.0 copy-done.7
  90.4 0.0 copy-done.8
  90.4 0.0 copy-done.9
  90.4 0.7 pad_maximum_fusion.1
  91.1 0.0 all-gather.5.cloned.1.call-update
  91.2 0.0 reduce-scatter.2.cloned.1.call-start
  91.2 37.3 %all-gather.7.cloned.1.call-done = bf16[1024,2048]{1,0:T(8,128)(2,1)} async-done(((bf16[1024,256]{1,0:T(8,128)(2,1)}), bf16[1024,2048]{1,0:T(8,128)(2,1)}) %all-gather.7.cloned.1.call-update) | async-done | bytes 4194320 | tf_op jit(solution)/shard_map/all_gather | solution.py:345
  128.5 3.1 %fusion = f32[1024]{0:T(1024)S(1)} fusion(bf16[1024,2048]{1,0:T(8,128)(2,1)} %all-gather.7.cloned.1.call-done), kind=kLoop, calls=%fused_computation.2 | loop fusion | flops 6290432 | bytes 4198400 | tf_op jit(solution)/shard_map/reduce_sum | solution.py:348
  131.6 94.6 %all-gather.5.cloned.1.call-done = bf16[2048,1920]{1,0:T(8,128)(2,1)} async-done(((bf16[64,1920]{1,0:T(8,128)(2,1)}), bf16[2048,1920]{1,0:T(8,128)(2,1)}) %all-gather.5.cloned.1.call-update) | async-done | bytes 7864336 | tf_op jit(solution)/shard_map/all_gather | solution.py:352
  226.2 0.0 copy-done.11
  226.2 8.0 %fusion.3 = f32[1024,640]{1,0:T(8,128)} fusion(bf16[2048,1920]{1,0:T(8,128)(2,1)} %all-gather.5.cloned.1.call-done, bf16[1024,2048]{1,0:T(8,128)(2,1)} %all-gather.7.cloned.1.call-done, f32[2048]{0:T(1024)S(1)} %copy-done.11, f32[1024]{0:T(1024)S(1)} %add_rsqrt_fusion), kind=kOutput, calls=%fused_computation.6 | convolution fusion | flops 2692743168 | bytes 9449472 | tf_op jit(solution)/shard_map/dot_general | solution.py:356
  234.2 13.1 %convolution_convert_fusion = bf16[2048,1024]{0,1:T(8,128)(2,1)} fusion(bf16[2048,1920]{1,0:T(8,128)(2,1)} %all-gather.5.cloned.1.call-done, f32[1024,640]{1,0:T(8,128)} %fusion.3, bf16[1024,2048]{1,0:T(8,128)(2,1)} %all-gather.7.cloned.1.call-done, f32[2048]{0:T(1024)S(1)} %copy-done.11, f32[1024]{0:T(1024)S(1)} %add_rsqrt_fusion), kind=kOutput, calls=%fused_computation.5 | convolution fusion | flops 5383127040 | bytes 16265216 | tf_op jit(solution)/shard_map/dot_general | solution.py:32
  247.3 0.0 copy-start.6
  247.3 0.0 reduce-scatter.2.cloned.1.call-update
  247.3 35.6 %reduce-scatter.2.cloned.1.call-done = bf16[256,1024]{0,1:T(8,128)(2,1)} async-done(((bf16[2048,1024]{0,1:T(8,128)(2,1)}), bf16[256,1024]{0,1:T(8,128)(2,1)}) %reduce-scatter.2.cloned.1.call-update) | async-done | bytes 524304 | tf_op jit(solution)/shard_map/reduce_scatter | solution.py:359
  283.0 0.0 copy-done.6
  283.0 2.0 fusion.14
  (7 shorter events, 0.1 us)
Async XLA Ops:
  6.5 79.5 %copy-start = (bf16[2,1024,256]{2,1,0:T(8,128)(2,1)S(1)}, bf16[2,1024,256]{2,1,0:T(8,128)(2,1)}, u32[]{:S(2)}) copy-start(bf16[2,1024,256]{2,1,0:T(8,128)(2,1)} %param.32) | copy-start | bytes 3145732
  6.5 79.5 %all-gather.9.cloned.1.call-start = ((), (), s32[]{:S(2)}) async-start(), calls=%async_computation.4 | async-start | bytes 4718592 | tf_op jit(solution)/shard_map/all_gather | solution.py:337
  12.0 1.0 copy-start.1
  13.0 0.9 copy-start.2
  13.9 0.7 copy-start.3
  14.6 0.7 copy-start.4
  15.3 0.7 copy-start.5
  16.0 70.1 %copy-start.10 = (bf16[1024,256]{1,0:T(8,128)(2,1)S(1)}, bf16[1024,256]{1,0:T(8,128)(2,1)}, u32[]{:S(2)}) copy-start(bf16[1024,256]{1,0:T(8,128)(2,1)} %param.33) | copy-start | bytes 1572868
  51.2 77.3 %all-gather.7.cloned.1.call-start = ((), (), s32[]{:S(2)}) async-start(), calls=%async_computation.2 | async-start | bytes 4718592 | tf_op jit(solution)/shard_map/all_gather | solution.py:345
  86.0 4.4 %copy-start.7 = (bf16[64,640]{1,0:T(8,128)(2,1)S(1)}, bf16[64,640]{1,0:T(8,128)(2,1)}, u32[]{:S(2)}) copy-start(bf16[64,640]{1,0:T(8,128)(2,1)} %param.37) | copy-start | bytes 245764
  86.0 4.4 %copy-start.8 = (bf16[64,640]{1,0:T(8,128)(2,1)S(1)}, bf16[64,640]{1,0:T(8,128)(2,1)}, u32[]{:S(2)}) copy-start(bf16[64,640]{1,0:T(8,128)(2,1)} %param.36) | copy-start | bytes 245764
  86.0 4.4 %copy-start.9 = (bf16[64,640]{1,0:T(8,128)(2,1)S(1)}, bf16[64,640]{1,0:T(8,128)(2,1)}, u32[]{:S(2)}) copy-start(bf16[64,640]{1,0:T(8,128)(2,1)} %param.35) | copy-start | bytes 245764
  90.3 135.9 %copy-start.11 = (f32[2048]{0:T(1024)S(1)}, f32[2048]{0:T(1024)}, u32[]{:S(2)}) copy-start(f32[2048]{0:T(1024)} %param.34) | copy-start | bytes 24580
  90.3 135.9 %all-gather.5.cloned.1.call-start = ((), (), s32[]{:S(2)}) async-start(), calls=%async_computation.1 | async-start | bytes 8110080 | tf_op jit(solution)/shard_map/all_gather | solution.py:352
  91.2 191.8 %reduce-scatter.2.cloned.1.call-start = ((), (), s32[]{:S(2)}) async-start(), calls=%async_computation.3 | async-start | bytes 4718592 | tf_op jit(solution)/shard_map/reduce_scatter | solution.py:359
  247.3 35.7 %copy-start.6 = (bf16[1024,256]{1,0:T(8,128)(2,1)S(1)}, bf16[1024,256]{1,0:T(8,128)(2,1)}, u32[]{:S(2)}) copy-start(bf16[1024,256]{1,0:T(8,128)(2,1)} %fusion.11) | copy-start | bytes 1572868
Sparse Core Ops, SparseCore 0:
  51.4 34.6 all-gather.8
  90.5 38.0 all-gather.6
  131.1 95.0 all-gather.4
  247.5 35.4 reduce-scatter.1

commit v2 on v1

--- a/solution.py
+++ b/solution.py
@@ -18,6 +18,10 @@
 NZ = 8
 QROWS = 48
 MROWS = 64
+NX = 4
+NTP = 8
+CHUNKS = 2
+N_PUT = 160
 
 
 def silu(v):
@@ -53,36 +57,147 @@
     return v[0:1] + v[2:3] + v[4:5], v[1:2] + v[3:4] + v[5:6]
 
 
-def front_kernel(
-    xs, gs, k1, q1, kq2, table, head_taps, taps1, taps2, gain,
-    mixed,
+class Net:
+    def __init__(self, send, recv):
+        self.send, self.recv, self.count, self.sent = send, recv, 0, []
+
+    def make(self, src, dst, to, index):
+        return pltpu.make_async_remote_copy(
+            src_ref=src, dst_ref=dst, send_sem=self.send.at[index], recv_sem=self.recv.at[index],
+            device_id=to, device_id_type=MESH)
+
+    def put(self, src, dst, to):
+        copy = self.make(src, dst, to, self.count)
+        self.count += 1
+        copy.start()
+        self.sent.append(copy)
+        return copy
+
+    def reserve(self, n):
+        at = self.count
+        self.count += n
+        return at
+
+
+def layer_kernel(
+    xs, gs, k1, q1, kq2, table, head_taps, taps1, taps2, gain, channel_gain,
+    out_w, resid, gate_w, up_w, down_w,
+    out,
     rim, keys, queries, values, local, cols, erun, state, starts,
     msg1, buf1, msg2, buf2, msg3, enter,
-    rim_send, rim_recv, send1, recv1, send2, recv2, send3, recv3,
+    gu, dn, wo, res, mix_send, mix, stm, feat, nb, hidden, ps, pr, po, relay_l, relay_r,
+    qs, from_l, from_r,
+    local_sem, send_sem, recv_sem,
 ):
     sp = lax.axis_index("sp")
+    tp = lax.axis_index("tp")
     y = lax.rem(sp, NY)
     z = sp // NY
+    core = lax.rem(tp, 2)
+    x = tp // 2
     n_sp = NY * NZ
     blocks = xs.shape[1] // BLOCK
+    width = gate_w.shape[1]
     right = lax.rem(sp + 1, n_sp)
     left = lax.rem(sp + n_sp - 1, n_sp)
-    y_peers = [z * NY + lax.rem(y + j, NY) for j in range(1, NY)]
-    z_peers = [lax.rem(z + j, NZ) * NY + y for j in range(1, NZ)]
+
+    def zmod(v):
+        return lax.rem(v + NZ, NZ)
+
+    def ymod(v):
+        return lax.rem(v + NY, NY)
+
+    y_peers = [{"sp": z * NY + ymod(y + j)} for j in range(1, NY)]
+    z_peers = [{"sp": zmod(z + j) * NY + y} for j in range(1, NZ)]
+    tp_peers = [{"tp": lax.rem(tp + j, NTP)} for j in range(1, NTP)]
+    up_y, down_y = {"sp": z * NY + ymod(y + 1)}, {"sp": z * NY + ymod(y - 1)}
+    up_z, down_z = {"sp": zmod(z + 1) * NY + y}, {"sp": zmod(z - 1) * NY + y}
+    slot_l = lax.rem(x + NX - 1, NX) * 2 + core
+    slot_r = lax.rem(x + 1, NX) * 2 + core
+    slot_o = lax.rem(x + 2, NX) * 2 + core
+    partner_slot = x * 2 + 1 - core
+    partner, x_right, x_left = {"tp": partner_slot}, {"tp": slot_r}, {"tp": slot_l}
+
+    own = [
+        pltpu.make_async_copy(gate_w, gu.at[z, y, :, 0:width], local_sem.at[0]),
+        pltpu.make_async_copy(up_w, gu.at[z, y, :, width:], local_sem.at[1]),
+        pltpu.make_async_copy(down_w, dn.at[z, y], local_sem.at[2]),
+        pltpu.make_async_copy(out_w, wo.at[tp], local_sem.at[3]),
+        pltpu.make_async_copy(resid.at[tp], res.at[tp], local_sem.at[4]),
+    ]
+    for copy in own:
+        copy.start()
 
     barrier = pltpu.get_barrier_semaphore()
-    for peer in [right, left] + y_peers + z_peers:
-        pl.semaphore_signal(barrier, inc=1, device_id={"sp": peer}, device_id_type=MESH)
-    pl.semaphore_wait(barrier, 2 + (NY - 1) + (NZ - 1))
-
+    greet = [{"sp": right}, {"sp": left}] + y_peers + z_peers + tp_peers
+    for peer in greet:
+        pl.semaphore_signal(barrier, inc=1, device_id=peer, device_id_type=MESH)
+    pl.semaphore_wait(barrier, len(greet))
+
+    net = Net(send_sem, recv_sem)
     tail = pl.ds(xs.shape[1] - 16, 16)
-    rim_copies = []
-    for n, src in enumerate([xs.at[0, tail], xs.at[1, tail], k1.at[tail], q1.at[tail], kq2.at[tail]]):
-        copy = pltpu.make_async_remote_copy(
-            src_ref=src, dst_ref=rim.at[n], send_sem=rim_send.at[n], recv_sem=rim_recv.at[n],
-            device_id={"sp": right}, device_id_type=MESH)
-        copy.start()
-        rim_copies.append(copy)
+    rims = [net.put(src, rim.at[n], {"sp": right}) for n, src in enumerate(
+        [xs.at[0, tail], xs.at[1, tail], k1.at[tail], q1.at[tail], kq2.at[tail]])]
+
+    def both(ref_a, ref_b, to_a, to_b):
+        return net.put(ref_a, ref_a, to_a), net.put(ref_b, ref_b, to_b)
+
+    def arrive(pair):
+        for copy in pair:
+            copy.wait_recv()
+
+    def gu_z(r):
+        a, b = zmod(z - (r - 1)), zmod(z + (r - 1))
+        if r == 4:
+            return both(gu.at[a, y, :, 0:width], gu.at[b, y, :, width:], up_z, down_z)
+        return both(gu.at[a, y], gu.at[b, y], up_z, down_z)
+
+    def gu_y(k):
+        zz = zmod(z + k)
+        return both(gu.at[zz, y], gu.at[zz, y], up_y, down_y)
+
+    def gu_y_relay(k):
+        zz = zmod(z + k)
+        return both(gu.at[zz, ymod(y - 1), :, 0:width], gu.at[zz, ymod(y + 1), :, width:], up_y, down_y)
+
+    def dn_z(r):
+        a, b = zmod(z - (r - 1)), zmod(z + (r - 1))
+        if r == 4:
+            return both(dn.at[a, 0:2], dn.at[b, 2:4], up_z, down_z)
+        return both(dn.at[a], dn.at[b], up_z, down_z)
+
+    def wo_first(g):
+        ref = wo.at[tp, g]
+        return net.put(ref, ref, x_right), net.put(ref, ref, x_left), net.put(ref, ref, partner)
+
+    def gather_second(ref_l, ref_r, half):
+        a, b = ref_l.at[0:half], ref_r.at[half:]
+        return (net.put(a, a, x_right), net.put(b, b, x_left),
+                net.put(ref_l, ref_l, partner), net.put(ref_r, ref_r, partner))
+
+    for copy in own[:3]:
+        copy.wait()
+    gz1 = gu_z(1)
+    gy = {0: gu_y(0)}
+    gr = {}
+    dy = both(dn.at[z, y], dn.at[z, y], up_y, down_y)
+    resid_puts = []
+    for j in range(1, NTP):
+        to = lax.rem(tp + j, NTP)
+        resid_puts.append(net.put(resid.at[to], res.at[tp], {"tp": to}))
+    own[3].wait()
+    own[4].wait()
+    wo_a = [wo_first(0), wo_first(1)]
+    wo_b, wo_c = [], []
+
+    def pump_wo(g):
+        arrive(wo_a[g][:2])
+        wo_b.append(gather_second(wo.at[slot_l, g], wo.at[slot_r, g], wo.shape[2] // 2))
+
+    def pump_wo_last(g):
+        arrive(wo_b[g][:2])
+        ref = wo.at[slot_o, g]
+        wo_c.append(net.put(ref, ref, partner))
 
     lane = lax.broadcasted_iota(jnp.int32, (8, 128), 1)
     row8 = lax.broadcasted_iota(jnp.int32, (8, 128), 0)
@@ -92,8 +207,8 @@
         jnp.int32, (BLOCK, BLOCK), 1)
 
     state[...] = jnp.zeros_like(state)
-    for copy in rim_copies:
-        copy.wait()
+    for copy in rims:
+        copy.wait_recv()
     has_left = sp > 0
     tails = tuple(
         jnp.where(has_left, rim[n].astype(F32)[8:16], 0.0) for n in range(5))
@@ -139,7 +254,16 @@
         offs = offs + jnp.broadcast_to(c[:, 127:128], (8, 128))
         return tuple(v[BLOCK - 8 :] for v in raw) + (offs,)
 
-    carry = lax.fori_loop(0, blocks, first, tails + (jnp.zeros((8, 128), F32),))
+    carry = lax.fori_loop(
+        0, blocks // 2, first, tails + (jnp.zeros((8, 128), F32),))
+
+    arrive(gz1)
+    gz2 = gu_z(2)
+    gy[1], gy[-1] = gu_y(1), gu_y(-1)
+    arrive(dy)
+    dy2 = both(dn.at[z, ymod(y - 1), 0:32], dn.at[z, ymod(y + 1), 32:64], up_y, down_y)
+
+    carry = lax.fori_loop(blocks // 2, blocks, first, carry)
     offs = carry[5]
     log0 = halves(low1, offs[0:1], offs[1:2])
     log1 = halves(low1, offs[2:3], offs[3:4])
@@ -151,13 +275,15 @@
         msg1[q, QROWS:MROWS] = logs
     copies1 = []
     for j in range(1, NY):
-        to = lax.rem(y + j, NY)
-        copy = pltpu.make_async_remote_copy(
-            src_ref=msg1.at[to], dst_ref=buf1.at[y], send_sem=send1.at[j - 1],
-            recv_sem=recv1.at[j - 1], device_id={"sp": z * NY + to}, device_id_type=MESH)
-        copy.start()
-        copies1.append(copy)
+        to = ymod(y + j)
+        copies1.append(net.put(msg1.at[to], buf1.at[y], {"sp": z * NY + to}))
     buf1[y] = msg1[y]
+
+    arrive(gz2)
+    gz3 = gu_z(3)
+    arrive(gy[0])
+    gr[0] = gu_y_relay(0)
+    pump_wo(0)
 
     def inside(b, carry):
         at = pl.ds(pl.multiple_of(b * BLOCK, BLOCK), BLOCK)
@@ -180,8 +306,7 @@
 
     lax.fori_loop(0, blocks // 2, inside, 0)
 
-    for copy in copies1:
-        copy.wait()
+    arrive(copies1)
     rows = y * QROWS + lax.broadcasted_iota(jnp.int32, (QROWS, 128), 0)
     group_one = rows < 128
 
@@ -202,18 +327,17 @@
     msg2[QROWS:MROWS] = log_rows(sum0, sum1)
     copies2 = []
     for j in range(1, NZ):
-        copy = pltpu.make_async_remote_copy(
-            src_ref=msg2, dst_ref=buf2.at[z], send_sem=send2.at[j - 1],
-            recv_sem=recv2.at[j - 1], device_id={"sp": lax.rem(z + j, NZ) * NY + y},
-            device_id_type=MESH)
-        copy.start()
-        copies2.append(copy)
+        copies2.append(net.put(msg2, buf2.at[z], {"sp": zmod(z + j) * NY + y}))
     buf2[z] = msg2[...]
 
+    arrive(gz3)
+    gz4 = gu_z(4)
+    arrive(dy2)
+    dz1 = dn_z(1)
+
     lax.fori_loop(blocks // 2, blocks, inside, 0)
 
-    for copy in copies2:
-        copy.wait()
+    arrive(copies2)
     run = jnp.zeros((QROWS, 128), F32)
     for j in range(NZ):
         l0, l1 = read_logs(buf2[j, QROWS:MROWS])
@@ -225,20 +349,29 @@
     mine = pl.ds(pl.multiple_of(y * QROWS, 16), QROWS)
     copies3 = []
     for j in range(1, NY):
-        to = lax.rem(y + j, NY)
-        copy = pltpu.make_async_remote_copy(
-            src_ref=msg3.at[to], dst_ref=enter.at[mine], send_sem=send3.at[j - 1],
-            recv_sem=recv3.at[j - 1], device_id={"sp": z * NY + to}, device_id_type=MESH)
-        copy.start()
-        copies3.append(copy)
+        to = ymod(y + j)
+        copies3.append(net.put(msg3.at[to], enter.at[mine], {"sp": z * NY + to}))
     enter[mine] = msg3[y]
-    for copy in copies3:
-        copy.wait()
+
+    gy[2], gy[-2] = gu_y(2), gu_y(-2)
+    arrive(gy[1])
+    gr[1] = gu_y_relay(1)
+    arrive(gy[-1])
+    gr[-1] = gu_y_relay(-1)
+    pump_wo(1)
+    arrive(copies3)
 
     enter_one = enter[0:128]
     enter_two = jnp.concatenate([enter[128:192], jnp.zeros((64, 128), BF16)], axis=0)
 
-    def finish(b, carry):
+    mix_at = net.reserve(NTP - 1)
+
+    def mix_copy(i):
+        to = lax.rem(tp + 1 + i, NTP)
+        return net.make(mix_send.at[to], mix.at[tp], {"tp": to}, mix_at + i)
+
+    def finish(i, carry):
+        b = lax.rem(tp + 1 + i, NTP)
         at = pl.ds(pl.multiple_of(b * BLOCK, BLOCK), BLOCK)
         e = erun[b]
         for g, entering in enumerate([enter_one, enter_two]):
@@ -250,21 +383,185 @@
             s0 = jnp.sum(jnp.where(low, square, 0.0), axis=1, keepdims=True)
             s1 = jnp.sum(jnp.where(low, 0.0, square), axis=1, keepdims=True)
             scale = lax.rsqrt(halves(low, s0, s1) * (1.0 / HEAD) + EPSILON)
-            mixed[g, at] = (m * scale * gain[g : g + 1]).astype(BF16)
+            mix_send[b, g] = (m * scale * gain[g : g + 1]).astype(BF16)
+
+        @pl.when(i < NTP - 1)
+        def _():
+            mix_copy(i).start()
+
         return carry
 
-    lax.fori_loop(0, blocks, finish, 0)
-
-
-def front(xs, gs, k1, q1, kq2, table, head_taps, taps1, taps2, gain):
-    length = xs.shape[1]
+    lax.fori_loop(0, NTP, finish, 0)
+    mix[tp] = mix_send[tp]
+
+    arrive(dz1)
+    dz2 = dn_z(2)
+    arrive(gz4)
+    gy[3], gy[-3] = gu_y(3), gu_y(-3)
+    gy[4] = gu_y(4)
+    pump_wo_last(0)
+    arrive(resid_puts)
+    pump_wo_last(1)
+    for i in range(NTP - 1):
+        mix_copy(i).wait_recv()
+    for g in range(2):
+        wo_a[g][2].wait_recv()
+        arrive(wo_b[g][2:])
+        wo_c[g].wait_recv()
+
+    lhs = jnp.concatenate([mix[t, g] for g in range(2) for t in range(NTP)], axis=1)
+    depth = lhs.shape[1]
+    square = jnp.zeros((BLOCK, 1), F32)
+    for s in range(NTP):
+        row = dot(lhs, wo[s].reshape(depth, 256), 1, 0) + res[s].astype(F32)
+        row = row.astype(BF16)
+        stm[s] = row
+        wide = row.astype(F32)
+        square = square + jnp.sum(wide * wide, axis=1, keepdims=True)
+    scale = lax.rsqrt(square * (1.0 / depth) + EPSILON)
+    tokens = BLOCK // CHUNKS
+    for s in range(NTP):
+        cut = slice(s * 256, (s + 1) * 256)
+        normed = (stm[s].astype(F32) * scale * channel_gain[:, cut]).astype(BF16)
+        for h in range(CHUNKS):
+            nb[h, tp, :, cut] = normed[h * tokens : (h + 1) * tokens]
+
+    arrive(dz2)
+    dz3 = dn_z(3)
+    ag_a, ag_b, ag_c = [], [], []
+    for h in range(CHUNKS):
+        ref = nb.at[h, tp]
+        ag_a.append((net.put(ref, ref, x_right), net.put(ref, ref, x_left), net.put(ref, ref, partner)))
+    arrive(gy[2])
+    gr[2] = gu_y_relay(2)
+    arrive(gy[-2])
+    gr[-2] = gu_y_relay(-2)
+
+    def ag_second(h):
+        arrive(ag_a[h][:2])
+        ag_b.append(gather_second(nb.at[h, slot_l], nb.at[h, slot_r], tokens // 2))
+
+    def ag_third(h):
+        arrive(ag_b[h][:2])
+        ref = nb.at[h, slot_o]
+        ag_c.append(net.put(ref, ref, partner))
+
+    def ag_done(h):
+        ag_a[h][2].wait_recv()
+        arrive(ag_b[h][2:])
+        ag_c[h].wait_recv()
+
+    ag_second(0)
+    arrive(gy[3])
+    gr[3] = gu_y_relay(3)
+    arrive(gy[-3])
+    gr[-3] = gu_y_relay(-3)
+    arrive(gy[4])
+    gr[4] = gu_y_relay(4)
+    arrive(dz3)
+    dz4 = dn_z(4)
+    ag_third(0)
+    feat_puts = []
+    ag_second(1)
+    for j in range(1, NTP):
+        to = lax.rem(tp + j, NTP)
+        feat_puts.append(net.put(stm.at[to], feat.at[tp], {"tp": to}))
+    feat[tp] = stm[tp]
+    for k in (0, 1, -1, 2, -2, 3, -3, 4):
+        arrive(gr[k])
+    ag_done(0)
+
+    n_rows = NTP * tokens
+    order = (2, 3, 1, 0)
+    dests = {k: lax.rem(x + k, NX) * 2 for k in order}
+
+    def hid(h):
+        for m in range(2):
+            rows_in = nb[h, 4 * m : 4 * m + 4].reshape(4 * tokens, depth)
+            both_up = dot(rows_in, gu[...].reshape(depth, 2 * width), 1, 0)
+            g, u = both_up[:, :width], both_up[:, width:]
+            hidden[4 * tokens * m : 4 * tokens * (m + 1)] = (silu(g) * u).astype(BF16)
+
+    def down(d):
+        return dot(hidden[...], dn[d].reshape(256, width), 1, 1).astype(BF16)
+
+    ps_puts, rl_puts, out_puts = {}, {}, {}
+
+    def down_partner(h):
+        for k in order:
+            ps[h, k] = down(dests[k] + 1 - core)
+            ps_puts[h, k] = net.put(ps.at[h, k], pr.at[h, k], partner)
+
+    def down_own(h):
+        for k in order:
+            po[h, k] = down(dests[k] + core)
+
+    def pair_sum(h, k):
+        ps_puts[h, k].wait_recv()
+        return po[h, k].astype(F32) + pr[h, k].astype(F32)
+
+    mid = n_rows // 2
+
+    def rs_first(h):
+        qs[h, 2] = pair_sum(h, 2).astype(BF16)
+        rl_puts[h] = (net.put(qs.at[h, 2, 0:mid], relay_r.at[h], x_left),
+                      net.put(qs.at[h, 2, mid:], relay_l.at[h], x_right))
+
+    def rs_second(h):
+        to_left, to_right = pair_sum(h, 3), pair_sum(h, 1)
+        arrive(rl_puts[h])
+        qs[h, 3, 0:mid] = (to_left[0:mid] + relay_r[h].astype(F32)).astype(BF16)
+        qs[h, 3, mid:] = to_left[mid:].astype(BF16)
+        qs[h, 1, 0:mid] = to_right[0:mid].astype(BF16)
+        qs[h, 1, mid:] = (to_right[mid:] + relay_l[h].astype(F32)).astype(BF16)
+        out_puts[h] = (net.put(qs.at[h, 3], from_r.at[h], x_left),
+                       net.put(qs.at[h, 1], from_l.at[h], x_right))
+
+    def rs_third(h):
+        total = pair_sum(h, 0)
+        arrive(out_puts[h])
+        total = total + from_l[h].astype(F32) + from_r[h].astype(F32)
+        at = slice(h * tokens, (h + 1) * tokens)
+        stream = feat[:, at].astype(F32)
+        out[:, at] = (stream + 0.5 * total.reshape(NTP, tokens, 256)).astype(BF16)
+
+    hid(0)
+    ag_third(1)
+    for pair in (dz4,):
+        arrive(pair)
+    down_partner(0)
+    down_own(0)
+    rs_first(0)
+    ag_done(1)
+    hid(1)
+    rs_second(0)
+    down_partner(1)
+    down_own(1)
+    rs_first(1)
+    arrive(feat_puts)
+    rs_third(0)
+    rs_second(1)
+    rs_third(1)
+
+    for copy in net.sent:
+        copy.wait_send()
+    for i in range(NTP - 1):
+        mix_copy(i).wait_send()
+
+
+def layer(args, hbm_args):
+    length = args[0].shape[1]
     blocks = length // BLOCK
+    tokens = BLOCK // CHUNKS
+    n_rows = NTP * tokens
     vmem = pl.BlockSpec(memory_space=pltpu.VMEM)
+    hbm = pl.BlockSpec(memory_space=pl.ANY)
     dma = pltpu.SemaphoreType.DMA
+    width = hbm_args[2].shape[1]
     return pl.pallas_call(
-        front_kernel,
-        out_shape=jax.ShapeDtypeStruct((2, length, 128), BF16),
-        in_specs=[vmem] * 10,
+        layer_kernel,
+        out_shape=jax.ShapeDtypeStruct((NTP, BLOCK, 256), BF16),
+        in_specs=[vmem] * len(args) + [hbm] * len(hbm_args),
         out_specs=vmem,
         scratch_shapes=[
             pltpu.VMEM((5, 16, 128), BF16),
@@ -282,17 +579,32 @@
             pltpu.VMEM((NZ, MROWS, 128), BF16),
             pltpu.VMEM((NY, QROWS, 128), BF16),
             pltpu.VMEM((NY * QROWS, 128), BF16),
-            dma((5,)), dma((5,)),
-            dma((NY - 1,)), dma((NY - 1,)),
-            dma((NZ - 1,)), dma((NZ - 1,)),
-            dma((NY - 1,)), dma((NY - 1,)),
+            pltpu.VMEM((NZ, NY, 64, 2 * width), BF16),
+            pltpu.VMEM((NZ, NY, 64, width), BF16),
+            pltpu.VMEM((NTP, 2, 1024, 256), BF16),
+            pltpu.VMEM((NTP, BLOCK, 256), BF16),
+            pltpu.VMEM((NTP, 2, BLOCK, 128), BF16),
+            pltpu.VMEM((NTP, 2, BLOCK, 128), BF16),
+            pltpu.VMEM((NTP, BLOCK, 256), BF16),
+            pltpu.VMEM((NTP, BLOCK, 256), BF16),
+            pltpu.VMEM((CHUNKS, NTP, tokens, 2048), BF16),
+            pltpu.VMEM((n_rows, width), BF16),
+            pltpu.VMEM((CHUNKS, NX, n_rows, 256), BF16),
+            pltpu.VMEM((CHUNKS, NX, n_rows, 256), BF16),
+            pltpu.VMEM((CHUNKS, NX, n_rows, 256), BF16),
+            pltpu.VMEM((CHUNKS, n_rows // 2, 256), BF16),
+            pltpu.VMEM((CHUNKS, n_rows // 2, 256), BF16),
+            pltpu.VMEM((CHUNKS, NX, n_rows, 256), BF16),
+            pltpu.VMEM((CHUNKS, n_rows, 256), BF16),
+            pltpu.VMEM((CHUNKS, n_rows, 256), BF16),
+            dma((5,)), dma((N_PUT,)), dma((N_PUT,)),
         ],
         compiler_params=pltpu.CompilerParams(
-            collective_id=0, has_side_effects=True, vmem_limit_bytes=24 * 1024 * 1024),
+            collective_id=0, has_side_effects=True, vmem_limit_bytes=58 * 1024 * 1024),
         cost_estimate=pl.CostEstimate(
-            flops=4_000_000_000, bytes_accessed=4_000_000, transcendentals=4_000_000),
-        name="front",
-    )(xs, gs, k1, q1, kq2, table, head_taps, taps1, taps2, gain)
+            flops=12_000_000_000, bytes_accessed=8_000_000, transcendentals=4_000_000),
+        name="layer",
+    )(*args, *hbm_args)
 
 
 def shards(
@@ -322,42 +634,29 @@
     log_decay = extra_log_decay - step * head_decay_rate[None]
     table = jnp.stack([log_decay, step]).reshape(2, blocks, BLOCK, 4)
     table = table.transpose(1, 0, 3, 2).reshape(blocks, 8, BLOCK)
-    mixed = front(
-        grouped_head_inputs.transpose(1, 0, 2),
-        head_gate_inputs.transpose(1, 0, 2),
-        first_group_keys,
-        first_group_queries,
-        jnp.concatenate([second_group_keys, second_group_queries], axis=1),
-        table,
-        head_input_filter,
-        first_group_filter,
-        second_group_filter.reshape(CONV, 128),
-        head_norm_gain,
+    out = layer(
+        (
+            grouped_head_inputs.transpose(1, 0, 2),
+            head_gate_inputs.transpose(1, 0, 2),
+            first_group_keys,
+            first_group_queries,
+            jnp.concatenate([second_group_keys, second_group_queries], axis=1),
+            table,
+            head_input_filter,
+            first_group_filter,
+            second_group_filter.reshape(CONV, 128),
+            head_norm_gain,
+            channel_norm_gain[None],
+        ),
+        (
+            output_weight,
+            residual.reshape(NTP, BLOCK, 256),
+            channel_gate_weight,
+            channel_up_weight,
+            channel_down_weight,
+        ),
     )
-    whole = lax.all_gather(mixed, "tp", axis=0)
-    projected = lax.dot_general(
-        whole,
-        output_weight.reshape(2, 8, 128, output_weight.shape[2]),
-        (((0, 1, 3), (1, 0, 2)), ((), ())),
-        preferred_element_type=F32,
-    )
-    stream = (residual.astype(F32) + projected).astype(BF16)
-    full_rows = lax.all_gather(stream, "tp", axis=1, tiled=True).astype(F32)
-    normed = (
-        full_rows
-        * lax.rsqrt(jnp.mean(full_rows * full_rows, axis=1, keepdims=True) + EPSILON)
-        * channel_norm_gain[None]
-    ).astype(BF16)
-    width = channel_gate_weight.shape[1]
-    weights = lax.all_gather(
-        jnp.concatenate([channel_gate_weight, channel_up_weight, channel_down_weight], axis=1),
-        "sp", axis=0, tiled=True)
-    gate = jnp.dot(normed, weights[:, :width], preferred_element_type=F32)
-    upward = jnp.dot(normed, weights[:, width : 2 * width], preferred_element_type=F32)
-    hidden = (jax.nn.silu(gate) * upward).astype(BF16)
-    partial = dot(weights[:, 2 * width :], hidden, 1, 1).astype(BF16)
-    summed = lax.psum_scatter(partial, "tp", scatter_dimension=0, tiled=True).astype(F32).T
-    return (stream.astype(F32) + 0.5 * summed).astype(BF16)
+    return out.reshape(length, 256)
 
 
 def solution(mesh):

time: 294 us -> 119 us (0.40)
  waiting for transfers between devices: 202 us -> 0 us
  Pallas kernels: 35.2 us -> 111 us
  matrix products: 25.4 us -> 0 us
  between operations: 13.3 us -> 0.05 us
  other arithmetic: 6.77 us -> 2.32 us
    all_gather x3 -> x0, waiting for transfers between devices: 167 us -> none  [the longest x1 94.6 us: shards(): lax.all_gather(jnp.concatenate([channel_gate_weight, channel_up_weight, c...]
    pallas_call x1, Pallas kernels: 35.2 us -> 111 us  [layer(): pl.pallas_call(layer_kernel, out_shape=jax.ShapeDtypeStruct((NTP, BLOCK,...]
    reduce_scatter x1 -> x0, waiting for transfers between devices: 35.6 us -> none  [shards(): lax.psum_scatter(partial, 'tp', scatter_dimension=0, tiled=True).astype(F32)]
    dot_general x3 -> x0, matrix products: 25.4 us -> none  [the longest x1 13.1 us: dot(): lax.dot_general(a, b, (((ca,), (cb,)), ((), ())), preferred_element_type=...]
    reduce_sum x1 -> x0, other arithmetic: 3.07 us -> none  [shards(): jnp.mean(full_rows * full_rows, axis=1, keepdims=True) + EPSILON]
    unnamed x26 -> x13, local copies, waits for them, and re-layouts: 6.15 us -> 3.1 us
  transfers between devices with their start and end apart: 4 -> 0, of which waited for: 4 -> 0; matrix products, arithmetic and copies ran while one was open for 1% -> 0% of each run, Pallas kernels for 0% -> 0%
where the time goes in v2:
time: 119 us
  Pallas kernels  111 us (93%)
  local copies, waits for them, and re-layouts  5.61 us (5%)
  other arithmetic  2.32 us (2%)
    pallas_call x1, Pallas kernels, layer(): pl.pallas_call(layer_kernel, out_shape=jax.ShapeDtypeStruct((NTP, BLOCK,...  111 us
    unnamed x13, local copies, waits for them, and re-layouts  3.1 us

profile of v2, /device:TPU:1, one launch (start us, length us, event | category | flops | bytes accessed | tf_op | source)
XLA Modules:
  0.0 118.7 jit_solution(16672963551251480606)
XLA Ops:
  0.0 0.0 copy-start.4
  0.0 1.4 %reshape.19.taps2 = f32[4,128]{1,0:T(4,128)} reshape(f32[4,2,64]{2,1,0:T(2,128)} %param.30) | data formatting | bytes 4096 | tf_op jit(solution)/shard_map/reshape | solution.py:647
  1.4 0.0 copy-done.4
  1.4 0.0 copy-start.2
  1.4 0.8 multiply_subtract_fusion
  2.3 0.6 pad_maximum_fusion.1
  2.9 0.0 copy-done.2
  2.9 0.0 copy-start.3
  2.9 0.2 copy.22
  3.1 0.7 copy-done.3
  3.8 0.0 copy-start
  3.8 0.0 copy-start.1
  3.8 0.2 copy.23
  4.0 0.9 pad_maximum_fusion.kq2
  4.8 0.0 copy-done
  4.8 0.2 copy-done.1
  5.0 1.1 copy_bitcast_fusion
  6.1 110.7 %layer.1 = bf16[8,128,256]{2,1,0:T(8,128)(2,1)} custom-call(bf16[2,1024,128]{2,1,0:T(8,128)(2,1)} %get-tuple-element.8.xs, bf16[2,1024,128]{2,1,0:T(8,128)(2,1)} %get-tuple-element.7.gs, bf16[1024,128]{1,0:T(8,128)(2,1)} %k1.1, bf16[1024,128]{1,0:T(8,128)(2,1)} %q1.1, bf16[1024,128]{1,0:T(8,128)(2,1)} %pad_maximum_fusion.kq2, f32[8,8,128]{2,1,0:T(8,128)} %bitcast.15, ...), custom_call_target="tpu_custom_call" | custom-call | flops 12000000000 | bytes 8000000 | tf_op jit(solution)/shard_map/layer/pallas_call | solution.py:561
  116.8 1.9 %copy.29 = bf16[1024,256]{1,0:T(8,128)(2,1)} copy(bf16[1024,256]{1,0:T(8,128)(2,1)} %bitcast.14) | data formatting | bytes 1048576
  (4 shorter events, 0.0 us)
Async XLA Ops:
  0.0 1.4 %copy-start.4 = (f32[2,2]{1,0:T(2,128)S(1)}, f32[2,2]{1,0:T(2,128)}, u32[]{:S(2)}) copy-start(f32[2,2]{1,0:T(2,128)} %param.22) | copy-start | bytes 52
  1.4 1.5 %copy-start.2 = (bf16[1024,64]{0,1:T(8,128)(2,1)S(1)}, bf16[1024,64]{0,1:T(8,128)(2,1)}, u32[]{:S(2)}) copy-start(bf16[1024,64]{0,1:T(8,128)(2,1)} %param.26) | copy-start | bytes 393220
  2.9 0.9 copy-start.3
  3.8 1.0 copy-start
  3.8 1.2 %copy-start.1 = (bf16[1024,2,128]{2,1,0:T(2,128)(2,1)S(1)}, bf16[1024,2,128]{2,1,0:T(2,128)(2,1)}, u32[]{:S(2)}) copy-start(bf16[1024,2,128]{2,1,0:T(2,128)(2,1)} %param.19) | copy-start | bytes 1572868

commit v3 on v1

v3 whole, which is shorter than its diff:
```python
import functools

import jax
import jax.numpy as jnp
from jax import lax
from jax.experimental import pallas as pl
from jax.experimental.pallas import tpu as pltpu
from jax.sharding import PartitionSpec as P

HEAD = 64
CONV = 4
BLOCK = 128
EPSILON = 1e-06
MESH = pl.DeviceIdType.MESH
F32 = jnp.float32
BF16 = jnp.bfloat16
NY = 4
NZ = 8
NX = 4
NTP = 8
QROWS = 48
MROWS = 64
CHUNKS = 4
N_PUT = 176
STEPS = (
    "bA", "bB", "b0", "s1", "gy1", "gz2", "ia", "ib", "s2", "dy2", "gz3", "dz1", "s3", "gy2",
    "gr-1", "gr0", "gr1", "gz4", "gy3", "fin0", "Ai0", "fin1", "Ai1", "fin2", "fin3", "gr2",
    "dz2", "Ai2", "Ar0", "gr-2", "gy4", "Ar1", "Ai3", "Ar2", "Af0", "Af1", "P0", "Bi0", "dz3",
    "P1", "Bi1", "gr3", "Ar3", "Af2", "gr-3", "P2", "Bi2", "Br0", "Br1", "dz4", "Af3", "gr4",
    "P3", "Bi3", "Br2", "Bf0", "Bf1", "H0", "D0", "H1", "Bf2", "Br3", "D1", "E0", "C10", "E1",
    "H2", "Bf3", "C11", "D2", "C20", "E2", "H3", "C12", "C21", "D3", "E3", "C30", "C13", "C22",
    "C31", "C23", "C32", "C33",
)


def mark(name):
    pass


def silu(v):
    return v * (0.5 * jnp.tanh(0.5 * v) + 0.5)


def halves(lane_low, a, b):
    return jnp.where(lane_low, a, b)


def dot(a, b, ca, cb):
    return lax.dot_general(a, b, (((ca,), (cb,)), ((), ())), preferred_element_type=F32)


def split_three(v):
    hi = v.astype(BF16)
    rest = v - hi.astype(F32)
    mid = rest.astype(BF16)
    low = (rest - mid.astype(F32)).astype(BF16)
    return hi, mid, low


def log_rows(l0, l1):
    rows = []
    for part0, part1 in zip(split_three(l0), split_three(l1)):
        rows += [part0.astype(F32), part1.astype(F32)]
    rows.append(jnp.zeros((10, 128), F32))
    return jnp.concatenate(rows, axis=0).astype(BF16)


def read_logs(rows):
    v = rows.astype(F32)
    return v[0:1] + v[2:3] + v[4:5], v[1:2] + v[3:4] + v[5:6]


class Net:
    def __init__(self, send, recv):
        self.send, self.recv, self.sent = send, recv, []

    def put(self, src, dst, to):
        index = len(self.sent)
        copy = pltpu.make_async_remote_copy(
            src_ref=src, dst_ref=dst, send_sem=self.send.at[index], recv_sem=self.recv.at[index],
            device_id=to, device_id_type=MESH)
        copy.start()
        self.sent.append(copy)
        return copy


def arrive(copies):
    for copy in copies:
        copy.wait_recv()


def layer_kernel(
    step_in, extra, head_taps, taps1, taps2, gain, channel_gain, rate,
    hx, hg, k1, q1, k2t, q2t, out_w, resid, gate_w, up_w, down_w,
    out,
    raw_x, raw_g, raw_k, raw_q, raw_t, xf, gf, pad, rim_x, rim_k, rim_q, rim_t,
    ctab, cols, keys, queries, values, local, gates, upd, starts,
    msg1, buf1, msg2, buf2, msg3, enter,
    gu, dn, wo, res, mx, st, nb, hidden, ps, pr, po, relay_l, relay_r, qs, from_l, from_r,
    local_sem, send_sem, recv_sem,
):
    sp = lax.axis_index("sp")
    tp = lax.axis_index("tp")
    y = lax.rem(sp, NY)
    z = sp // NY
    core = lax.rem(tp, 2)
    x = tp // 2
    n_sp = NY * NZ
    length = k1.shape[0]
    blocks = length // BLOCK
    width = gate_w.shape[1]
    depth = wo.shape[0]
    right = lax.rem(sp + 1, n_sp)
    left = lax.rem(sp + n_sp - 1, n_sp)

    def zmod(v):
        return lax.rem(v + NZ, NZ)

    def ymod(v):
        return lax.rem(v + NY, NY)

    y_peers = [{"sp": z * NY + ymod(y + j)} for j in range(1, NY)]
    z_peers = [{"sp": zmod(z + j) * NY + y} for j in range(1, NZ)]
    up_y, down_y = {"sp": z * NY + ymod(y + 1)}, {"sp": z * NY + ymod(y - 1)}
    up_z, down_z = {"sp": zmod(z + 1) * NY + y}, {"sp": zmod(z - 1) * NY + y}
    slot_l = lax.rem(x + NX - 1, NX) * 2 + core
    slot_r = lax.rem(x + 1, NX) * 2 + core
    slot_o = lax.rem(x + 2, NX) * 2 + core
    partner, x_right, x_left = {"tp": x * 2 + 1 - core}, {"tp": slot_r}, {"tp": slot_l}

    mark("barrier")
    wanted = [
        (gate_w, gu.at[z, y, :, 0:width]),
        (up_w, gu.at[z, y, :, width:]),
        (down_w, dn.at[z, y]),
        (hx, raw_x),
        (k1, raw_k),
        (q1, raw_q),
        (k2t, raw_t.at[0:64]),
        (q2t, raw_t.at[64:128]),
        (hg, raw_g),
        (out_w, wo),
        (resid, res),
    ]
    own = [pltpu.make_async_copy(a, b, local_sem.at[n]) for n, (a, b) in enumerate(wanted)]
    for copy in own:
        copy.start()

    barrier = pltpu.get_barrier_semaphore()
    greet = [{"sp": right}, {"sp": left}] + y_peers + z_peers + [partner, x_right, x_left]
    for peer in greet:
        pl.semaphore_signal(barrier, inc=1, device_id=peer, device_id_type=MESH)

    mark("tables")
    row8 = lax.broadcasted_iota(jnp.int32, (8, 128), 0)
    low = lax.broadcasted_iota(jnp.int32, (BLOCK, 128), 1) < HEAD
    low1 = lax.broadcasted_iota(jnp.int32, (1, 128), 1) < HEAD
    at_row = lax.broadcasted_iota(jnp.int32, (BLOCK, BLOCK), 0)
    at_col = lax.broadcasted_iota(jnp.int32, (BLOCK, BLOCK), 1)
    causal = at_row >= at_col
    upper = jnp.where(at_row <= at_col, 1.0, 0.0).astype(BF16)
    first_head = lax.broadcasted_iota(jnp.int32, (2, length), 0) == 0
    steps = [jax.nn.softplus(step_in[g]) for g in range(2)]
    logs = [extra[g] - steps[g] * jnp.where(first_head, rate[g, 0], rate[g, 1]) for g in range(2)]
    table = jnp.concatenate(
        [v[:, b * BLOCK : (b + 1) * BLOCK] for b in range(blocks) for v in logs + steps], axis=0)
    rows = table.shape[0]
    sums = dot(jnp.concatenate(split_three(table), axis=0), upper, 1, 0)
    sums = sums[0:rows] + sums[rows : 2 * rows] + sums[2 * rows :]
    offs = jnp.zeros((8, 1), F32)
    for b in range(blocks):
        cut = slice(8 * b, 8 * b + 8)
        c8 = jnp.where(row8 < 4, sums[cut], table[cut])
        ctab[b] = c8
        e8 = jnp.exp(jnp.where(row8 < 4, c8 + offs, 0.0))
        cols[b] = jnp.concatenate([c8, e8], axis=0).T
        offs = offs + c8[:, 127:128]
    log0 = halves(low1, offs[0:1], offs[1:2])
    log1 = halves(low1, offs[2:3], offs[3:4])
    my_logs = log_rows(log0, log1)
    for q in range(NY):
        msg1[q, QROWS:MROWS] = my_logs

    mark("barwait")
    for copy in own[:8]:
        copy.wait()
    pl.semaphore_wait(barrier, len(greet))

    net = Net(send_sem, recv_sem)
    got = {}
    have = {("gz", 0)}

    def need(*key):
        if key not in have:
            have.add(key)
            arrive(got[key])

    tail = pl.ds(length - 16, 16)
    rims = [
        net.put(raw_x.at[pl.ds(2 * length - 16, 16)], rim_x, {"sp": right}),
        net.put(raw_k.at[tail], rim_k, {"sp": right}),
        net.put(raw_q.at[tail], rim_q, {"sp": right}),
        net.put(raw_t.at[:, pl.ds(length - BLOCK, BLOCK)], rim_t, {"sp": right}),
    ]

    def both(ref_a, ref_b, to_a, to_b):
        return net.put(ref_a, ref_a, to_a), net.put(ref_b, ref_b, to_b)

    def gu_z(r):
        need("gz", r - 1)
        a, b = zmod(z - (r - 1)), zmod(z + (r - 1))
        if r == 4:
            got["gz", r] = both(gu.at[a, y, :, 0:width], gu.at[b, y, :, width:], up_z, down_z)
        else:
            got["gz", r] = both(gu.at[a, y], gu.at[b, y], up_z, down_z)

    def gu_y(*ks):
        for k in ks:
            need("gz", abs(k))
            zz = zmod(z + k)
            got["gy", k] = both(gu.at[zz, y], gu.at[zz, y], up_y, down_y)

    def gu_y_relay(k):
        arrive(got["gy", k])
        zz = zmod(z + k)
        got["gr", k] = both(
            gu.at[zz, ymod(y - 1), :, 0:width], gu.at[zz, ymod(y + 1), :, width:], up_y, down_y)

    def dn_y(r):
        if r == 1:
            got["dy", 1] = both(dn.at[z, y], dn.at[z, y], up_y, down_y)
        else:
            arrive(got["dy", 1])
            got["dy", 2] = both(
                dn.at[z, ymod(y - 1), 0:32], dn.at[z, ymod(y + 1), 32:64], up_y, down_y)

    def dn_z(r):
        arrive(got["dz", r - 1] if r > 1 else got["dy", 2])
        a, b = zmod(z - (r - 1)), zmod(z + (r - 1))
        if r == 4:
            got["dz", r] = both(dn.at[a, 0:2], dn.at[b, 2:4], up_z, down_z)
        else:
            got["dz", r] = both(dn.at[a], dn.at[b], up_z, down_z)

    def tp_first(buf, key, k):
        ref = buf.at[k, tp]
        got[key, k, 0] = (net.put(ref, ref, x_right), net.put(ref, ref, x_left))
        got[key, k, 1] = [net.put(ref, ref, partner)]

    def tp_second(buf, key, k):
        arrive(got[key, k, 0])
        ref_l, ref_r = buf.at[k, slot_l], buf.at[k, slot_r]
        half = buf.shape[2] // 2
        a, b = ref_l.at[0:half], ref_r.at[half:]
        got[key, k, 2] = (net.put(a, a, x_right), net.put(b, b, x_left))
        got[key, k, 1] += [net.put(ref_l, ref_l, partner), net.put(ref_r, ref_r, partner)]

    def tp_third(buf, key, k):
        arrive(got[key, k, 2])
        ref = buf.at[k, slot_o]
        got[key, k, 1] += [net.put(ref, ref, partner)]

    def tp_done(key, k):
        arrive(got[key, k, 1])

    mark("start")
    gu_z(1)
    gu_y(0)
    dn_y(1)

    mark("spread")
    xf[...] = raw_x[...].astype(F32)
    for g in range(2):
        pad[g, 8 : 8 + length] = xf[pl.ds(g, length, stride=2)]
    pad[2, 8 : 8 + length] = raw_k[...].astype(F32)
    pad[3, 8 : 8 + length] = raw_q[...].astype(F32)
    for b in range(blocks):
        pad[4, 8 + b * BLOCK : 8 + (b + 1) * BLOCK] = raw_t[:, b * BLOCK : (b + 1) * BLOCK].astype(F32).T
    second_taps = [jnp.concatenate([taps2[k, 0:1], taps2[k, 1:2]], axis=1) for k in range(CONV)]
    all_taps = [
        [head_taps[k, 0:1] for k in range(CONV)],
        [head_taps[k, 1:2] for k in range(CONV)],
        [taps1[k, 0:1] for k in range(CONV)],
        [taps1[k, 1:2] for k in range(CONV)],
        second_taps,
    ]

    def conv(n, b):
        full = pad[n, pl.ds(pl.multiple_of(b * BLOCK, BLOCK), BLOCK + 8)]
        taps = all_taps[n]
        total = taps[0] * full[5 : 5 + BLOCK]
        for k in range(1, CONV):
            total = total + taps[k] * full[5 + k : 5 + k + BLOCK]
        return silu(total)

    def block(b, carry):
        at = pl.ds(pl.multiple_of(b * BLOCK, BLOCK), BLOCK)
        c = ctab[b]
        t = cols[b]
        key_one, query_one, mix_two = conv(2, b), conv(3, b), conv(4, b)
        key_two = jnp.where(low, mix_two, 0.0)
        query_two = jnp.where(low, pltpu.roll(mix_two, 64, 1), 0.0)
        for g, (key, query) in enumerate([(key_one, query_one), (key_two, query_two)]):
            h = 2 * g
            v = conv(g, b) * halves(low, t[:, 4 + h : 5 + h], t[:, 5 + h : 6 + h])
            cum = halves(low, t[:, h : h + 1], t[:, h + 1 : h + 2])
            total = halves(low1, c[h : h + 1, 127:128], c[h + 1 : h + 2, 127:128])
            kb = key.astype(BF16)
            keys[g, at] = kb
            queries[g, at] = query.astype(BF16)
            values[g, at] = v.astype(BF16)
            upd[g, b] = dot(kb, (v * jnp.exp(total - cum)).astype(BF16), 0, 0)
        return carry

    def run_blocks(lo, hi):
        lax.fori_loop(lo, hi, block, 0, unroll=2)

    def last_block():
        block(blocks - 1, 0)
        arrive(rims)
        has_left = sp > 0
        xf[0:16] = rim_x[...].astype(F32)
        for g in range(2):
            pad[g, 0:8] = jnp.where(has_left, xf[pl.ds(g, 8, stride=2)], 0.0)
        pad[2, 0:8] = jnp.where(has_left, rim_k[...].astype(F32)[8:16], 0.0)
        pad[3, 0:8] = jnp.where(has_left, rim_q[...].astype(F32)[8:16], 0.0)
        pad[4, 0:8] = jnp.where(has_left, rim_t[...].astype(F32).T[BLOCK - 8 :], 0.0)
        block(0, 0)
        ends = []
        for g in range(2):
            h = 2 * g
            state = jnp.zeros((BLOCK, 128), F32)
            for b in range(blocks):
                c = ctab[b]
                total = halves(low1, c[h : h + 1, 127:128], c[h + 1 : h + 2, 127:128])
                starts[g, b] = state.astype(BF16)
                state = state * jnp.exp(total) + upd[g, b]
            ends.append(state)
        full = jnp.concatenate([ends[0], ends[1][0:64]], axis=0).astype(BF16)
        for q in range(NY):
            msg1[q, 0:QROWS] = full[q * QROWS : (q + 1) * QROWS]

    quarter = y * QROWS + lax.broadcasted_iota(jnp.int32, (QROWS, 128), 0)
    group_one = quarter < 128

    def factor(l0, l1):
        return jnp.where(group_one, jnp.exp(l0), jnp.exp(l1))

    def stage1():
        got["s1"] = []
        for j in range(1, NY):
            to = ymod(y + j)
            got["s1"].append(net.put(msg1.at[to], buf1.at[y], {"sp": z * NY + to}))
        buf1[y] = msg1[y]

    before = []

    def stage2():
        arrive(got["s1"])
        run = jnp.zeros((QROWS, 128), F32)
        sum0 = jnp.zeros((1, 128), F32)
        sum1 = jnp.zeros((1, 128), F32)
        for j in range(NY):
            before.append((run, sum0, sum1))
            l0, l1 = read_logs(buf1[j, QROWS:MROWS])
            run = run * factor(l0, l1) + buf1[j, 0:QROWS].astype(F32)
            sum0, sum1 = sum0 + l0, sum1 + l1
        msg2[0:QROWS] = run.astype(BF16)
        msg2[QROWS:MROWS] = log_rows(sum0, sum1)
        got["s2"] = []
        for j in range(1, NZ):
            got["s2"].append(net.put(msg2, buf2.at[z], {"sp": zmod(z + j) * NY + y}))
        buf2[z] = msg2[...]

    def stage3():
        arrive(got["s2"])
        run = jnp.zeros((QROWS, 128), F32)
        for j in range(NZ):
            l0, l1 = read_logs(buf2[j, QROWS:MROWS])
            new = run * factor(l0, l1) + buf2[j, 0:QROWS].astype(F32)
            run = jnp.where(j < z, new, run)
        for j in range(NY):
            part, l0, l1 = before[j]
            msg3[j] = (run * factor(l0, l1) + part).astype(BF16)
        mine = pl.ds(pl.multiple_of(y * QROWS, 16), QROWS)
        got["s3"] = []
        for j in range(1, NY):
            to = ymod(y + j)
            got["s3"].append(net.put(msg3.at[to], enter.at[mine], {"sp": z * NY + to}))
        enter[mine] = msg3[y]

    def inside(b, carry):
        at = pl.ds(pl.multiple_of(b * BLOCK, BLOCK), BLOCK)
        t = cols[b]
        c = ctab[b]
        for g in range(2):
            h = 2 * g
            qb, v = queries[g, at], values[g, at]
            scores = dot(qb, keys[g, at], 1, 1)
            weights = []
            for j in range(2):
                span = t[:, h + j : h + j + 1] - c[h + j : h + j + 1]
                weights.append((jnp.exp(jnp.where(causal, span, -jnp.inf)) * scores).astype(BF16))
            zero = jnp.zeros_like(v)
            two = jnp.concatenate([jnp.where(low, v, zero), jnp.where(low, zero, v)], axis=0)
            cum = halves(low, t[:, h : h + 1], t[:, h + 1 : h + 2])
            local[g, at] = dot(jnp.concatenate(weights, axis=1), two, 1, 0) + dot(
                qb, starts[g, b], 1, 0) * jnp.exp(cum)
        return carry

    def inside_a():
        own[8].wait()
        gf[...] = raw_g[...].astype(F32)
        for g in range(2):
            gates[g] = silu(gf[pl.ds(g, length, stride=2)])
        lax.fori_loop(0, blocks // 2, inside, 0, unroll=2)

    def inside_b():
        lax.fori_loop(blocks // 2, blocks, inside, 0, unroll=2)

    per = blocks // CHUNKS
    tokens = BLOCK * per

    def finish(k):
        if k == 0:
            arrive(got["s3"])
        for i in range(per):
            b = k * per + i
            at = slice(b * BLOCK, (b + 1) * BLOCK)
            t = cols[b]
            for g in range(2):
                h = 8 + 2 * g
                if g == 0:
                    entering = enter[0:128]
                else:
                    entering = jnp.concatenate([enter[128:192], jnp.zeros((64, 128), BF16)], axis=0)
                m = local[g, at] + dot(queries[g, at], entering, 1, 0) * halves(
                    low, t[:, h : h + 1], t[:, h + 1 : h + 2])
                m = m * gates[g, at]
                square = m * m
                s0 = jnp.sum(jnp.where(low, square, 0.0), axis=1, keepdims=True)
                s1 = jnp.sum(jnp.where(low, 0.0, square), axis=1, keepdims=True)
                scale = lax.rsqrt(halves(low, s0, s1) * (1.0 / HEAD) + EPSILON)
                mx[k, tp, i * BLOCK : (i + 1) * BLOCK, g * 128 : (g + 1) * 128] = (
                    m * scale * gain[g : g + 1]).astype(BF16)

    def project(k):
        if k == 0:
            own[9].wait()
            own[10].wait()
        tp_done("A", k)
        lhs = jnp.concatenate(
            [mx[k, s, :, g * 128 : (g + 1) * 128] for g in range(2) for s in range(NTP)], axis=1)
        row = dot(lhs, wo[...], 1, 0) + res[k * tokens : (k + 1) * tokens].astype(F32)
        st[k, tp] = row.astype(BF16)

    def norm_hidden(k):
        tp_done("B", k)
        if k == 0:
            for j in (0, 1, -1, 2, -2, 3, -3, 4):
                arrive(got["gr", j])
        square = jnp.zeros((tokens, 128), F32)
        for s in range(NTP):
            v = st[k, s].astype(F32)
            square = square + v[:, :128] * v[:, :128] + v[:, 128:] * v[:, 128:]
        scale = lax.rsqrt(jnp.sum(square, axis=1, keepdims=True) * (1.0 / depth) + EPSILON)
        for s in range(NTP):
            cut = slice(s * 256, (s + 1) * 256)
            nb[:, cut] = (st[k, s].astype(F32) * scale * channel_gain[:, cut]).astype(BF16)
        pair = dot(nb[...], gu[...].reshape(depth, 2 * width), 1, 0)
        hidden[k] = (silu(pair[:, :width]) * pair[:, width:]).astype(BF16)

    order = (2, 3, 1, 0)
    dests = {k: lax.rem(x + k, NX) * 2 for k in order}

    def down(k, d):
        return dot(hidden[k], dn[d].reshape(256, width), 1, 1).astype(BF16)

    def down_partner(k):
        if k == 0:
            arrive(got["dz", 4])
        for j in order:
            ps[k, j] = down(k, dests[j] + 1 - core)
            got["P", k, j] = net.put(ps.at[k, j], pr.at[k, j], partner)

    def down_own(k):
        for j in order:
            po[k, j] = down(k, dests[j] + core)

    def pair_sum(k, j):
        got["P", k, j].wait_recv()
        return po[k, j].astype(F32) + pr[k, j].astype(F32)

    mid = tokens // 2

    def sum_first(k):
        qs[k, 2] = pair_sum(k, 2).astype(BF16)
        got["C1", k] = (net.put(qs.at[k, 2, 0:mid], relay_r.at[k], x_left),
                        net.put(qs.at[k, 2, mid:], relay_l.at[k], x_right))

    def sum_second(k):
        to_left, to_right = pair_sum(k, 3), pair_sum(k, 1)
        arrive(got["C1", k])
        qs[k, 3, 0:mid] = (to_left[0:mid] + relay_r[k].astype(F32)).astype(BF16)
        qs[k, 3, mid:] = to_left[mid:].astype(BF16)
        qs[k, 1, 0:mid] = to_right[0:mid].astype(BF16)
        qs[k, 1, mid:] = (to_right[mid:] + relay_l[k].astype(F32)).astype(BF16)
        got["C2", k] = (net.put(qs.at[k, 3], from_r.at[k], x_left),
                        net.put(qs.at[k, 1], from_l.at[k], x_right))

    def sum_third(k):
        total = pair_sum(k, 0)
        arrive(got["C2", k])
        total = total + from_l[k].astype(F32) + from_r[k].astype(F32)
        out[k * tokens : (k + 1) * tokens] = (st[k, tp].astype(F32) + 0.5 * total).astype(BF16)

    run = {
        "bA": lambda: run_blocks(1, 5),
        "bB": lambda: run_blocks(5, 7),
        "b0": last_block,
        "s1": stage1,
        "s2": stage2,
        "s3": stage3,
        "ia": inside_a,
        "ib": inside_b,
        "gy1": lambda: gu_y(1, -1),
        "gy2": lambda: gu_y(2, -2),
        "gy3": lambda: gu_y(3, -3),
        "gy4": lambda: gu_y(4),
        "dy2": lambda: dn_y(2),
    }
    for r in (2, 3, 4):
        run[f"gz{r}"] = functools.partial(gu_z, r)
    for r in (1, 2, 3, 4):
        run[f"dz{r}"] = functools.partial(dn_z, r)
    for k in (0, 1, -1, 2, -2, 3, -3, 4):
        run[f"gr{k}"] = functools.partial(gu_y_relay, k)
    for k in range(CHUNKS):
        run[f"fin{k}"] = functools.partial(finish, k)
        run[f"P{k}"] = functools.partial(project, k)
        run[f"H{k}"] = functools.partial(norm_hidden, k)
        run[f"D{k}"] = functools.partial(down_partner, k)
        run[f"E{k}"] = functools.partial(down_own, k)
        run[f"C1{k}"] = functools.partial(sum_first, k)
        run[f"C2{k}"] = functools.partial(sum_second, k)
        run[f"C3{k}"] = functools.partial(sum_third, k)
        for key, buf in (("A", mx), ("B", st)):
            run[f"{key}i{k}"] = functools.partial(tp_first, buf, key, k)
            run[f"{key}r{k}"] = functools.partial(tp_second, buf, key, k)
            run[f"{key}f{k}"] = functools.partial(tp_third, buf, key, k)
    for name in STEPS:
        mark(name)
        run.pop(name)()
    assert not run

    mark("sends")
    for copy in net.sent:
        copy.wait_send()


def layer(vmem_args, smem_arg, hbm_args):
    length = hbm_args[2].shape[0]
    blocks = length // BLOCK
    tokens = length // CHUNKS
    width = hbm_args[8].shape[1]
    vmem = pl.BlockSpec(memory_space=pltpu.VMEM)
    dma = pltpu.SemaphoreType.DMA

    def bf(*shape):
        return pltpu.VMEM(shape, BF16)

    def fl(*shape):
        return pltpu.VMEM(shape, F32)

    return pl.pallas_call(
        layer_kernel,
        out_shape=jax.ShapeDtypeStruct((length, 256), BF16),
        in_specs=[vmem] * len(vmem_args)
        + [pl.BlockSpec(memory_space=pltpu.SMEM)]
        + [pl.BlockSpec(memory_space=pl.ANY)] * len(hbm_args),
        out_specs=vmem,
        scratch_shapes=[
            bf(2 * length, 128), bf(2 * length, 128), bf(length, 128), bf(length, 128),
            bf(128, length), fl(2 * length, 128), fl(2 * length, 128), fl(5, length + 8, 128),
            bf(16, 128), bf(16, 128), bf(16, 128), bf(128, 128),
            fl(blocks, 8, 128), fl(blocks, BLOCK, 16),
            bf(2, length, 128), bf(2, length, 128), bf(2, length, 128),
            fl(2, length, 128), fl(2, length, 128),
            fl(2, blocks, 128, 128), bf(2, blocks, 128, 128),
            bf(NY, MROWS, 128), bf(NY, MROWS, 128), bf(MROWS, 128), bf(NZ, MROWS, 128),
            bf(NY, QROWS, 128), bf(NY * QROWS, 128),
            bf(NZ, NY, 64, 2 * width), bf(NZ, NY, 64, width), bf(2048, 256), bf(length, 256),
            bf(CHUNKS, NTP, tokens, 256), bf(CHUNKS, NTP, tokens, 256),
            bf(tokens, 2048), bf(CHUNKS, tokens, width),
            bf(CHUNKS, NX, tokens, 256), bf(CHUNKS, NX, tokens, 256), bf(CHUNKS, NX, tokens, 256),
            bf(CHUNKS, tokens // 2, 256), bf(CHUNKS, tokens // 2, 256),
            bf(CHUNKS, NX, tokens, 256), bf(CHUNKS, tokens, 256), bf(CHUNKS, tokens, 256),
            dma((11,)), dma((N_PUT,)), dma((N_PUT,)),
        ],
        compiler_params=pltpu.CompilerParams(
            collective_id=0, has_side_effects=True, vmem_limit_bytes=58 * 1024 * 1024),
        cost_estimate=pl.CostEstimate(
            flops=12_000_000_000, bytes_accessed=8_000_000, transcendentals=4_000_000),
        name="layer",
    )(*vmem_args, smem_arg, *hbm_args)


def shards(
    grouped_head_inputs,
    head_gate_inputs,
    unsmoothed_step,
    head_decay_rate,
    extra_log_decay,
    first_group_keys,
    first_group_queries,
    second_group_keys,
    second_group_queries,
    head_input_filter,
    first_group_filter,
    second_group_filter,
    head_norm_gain,
    output_weight,
    residual,
    channel_norm_gain,
    channel_gate_weight,
    channel_up_weight,
    channel_down_weight,
):
    length = grouped_head_inputs.shape[0]
    return layer(
        (
            unsmoothed_step.transpose(1, 2, 0),
            extra_log_decay.transpose(1, 2, 0),
            head_input_filter,
            first_group_filter,
            second_group_filter,
            head_norm_gain,
            channel_norm_gain[None],
        ),
        head_decay_rate,
        (
            grouped_head_inputs.reshape(2 * length, 128),
            head_gate_inputs.reshape(2 * length, 128),
            first_group_keys,
            first_group_queries,
            second_group_keys.T,
            second_group_queries.T,
            output_weight.reshape(-1, output_weight.shape[2]),
            residual,
            channel_gate_weight,
            channel_up_weight,
            channel_down_weight,
        ),
    )


def solution(mesh):
    return jax.shard_map(
        shards,
        mesh=mesh,
        in_specs=(
            P("sp", None, "tp"),
            P("sp", None, "tp"),
            P("sp", None, "tp"),
            P(None, "tp"),
            P("sp", None, "tp"),
            P("sp", None),
            P("sp", None),
            P("sp", None),
            P("sp", None),
            P(None, None, "tp"),
            P(),
            P(),
            P(None, "tp"),
            P(None, None, "tp"),
            P("sp", "tp"),
            P(),
            P("sp", "tp"),
            P("sp", "tp"),
            P("sp", "tp"),
        ),
        out_specs=P("sp", "tp"),
        check_vma=False,
    )
```

time: 294 us -> 96.9 us (0.33)
  waiting for transfers between devices: 202 us -> 0 us
  Pallas kernels: 35.2 us -> 94.9 us
  matrix products: 25.4 us -> 0 us
  between operations: 13.3 us -> 0.01 us
  other arithmetic: 6.77 us -> 0 us
  local copies, waits for them, and re-layouts: 8.39 us -> 1.87 us
    all_gather x3 -> x0, waiting for transfers between devices: 167 us -> none  [the longest x1 94.6 us: shards(): lax.all_gather(jnp.concatenate([channel_gate_weight, channel_up_weight, c...]
    pallas_call x1, Pallas kernels: 35.2 us -> 94.9 us  [layer(): pl.pallas_call(layer_kernel, out_shape=jax.ShapeDtypeStruct((length, 256)...]
    reduce_scatter x1 -> x0, waiting for transfers between devices: 35.6 us -> none  [shards(): lax.psum_scatter(partial, 'tp', scatter_dimension=0, tiled=True).astype(F32)]
    dot_general x3 -> x0, matrix products: 25.4 us -> none  [the longest x1 13.1 us: dot(): lax.dot_general(a, b, (((ca,), (cb,)), ((), ())), preferred_element_type=...]
    unnamed x26 -> x1, local copies, waits for them, and re-layouts: 6.15 us -> 1.87 us
    reduce_sum x1 -> x0, other arithmetic: 3.07 us -> none  [shards(): jnp.mean(full_rows * full_rows, axis=1, keepdims=True) + EPSILON]
  transfers between devices with their start and end apart: 4 -> 0, of which waited for: 4 -> 0; matrix products, arithmetic and copies ran while one was open for 1% -> 0% of each run, Pallas kernels for 0% -> 0%
where the time goes in v3:
time: 96.9 us; the launch traced here: 96.7 us
  Pallas kernels  94.9 us (98%)
  local copies, waits for them, and re-layouts  1.87 us (2%)
    pallas_call x1, Pallas kernels, layer(): pl.pallas_call(layer_kernel, out_shape=jax.ShapeDtypeStruct((length, 256)...  94.9 us

profile of v3, /device:TPU:1, one launch (start us, length us, event | category | flops | bytes accessed | tf_op | source)
XLA Modules:
  0.0 96.7 jit_solution(9425514791489776735)
XLA Ops:
  0.0 94.9 %layer.1 = bf16[1024,256]{1,0:T(8,128)(2,1)} custom-call(f32[2,2,1024]{2,1,0:T(2,128)} %bitcast.13, f32[2,2,1024]{2,1,0:T(2,128)} %bitcast.14, f32[4,2,128]{2,1,0:T(2,128)} %head_taps.1, f32[4,2,128]{2,1,0:T(2,128)} %taps1.1, f32[4,2,64]{2,1,0:T(2,128)} %taps2.1, f32[2,128]{1,0:T(2,128)} %gain.1, f32[1,2048]{1,0:T(1,128)} %bitcast.15, f32[2,2]{1,0:T(2,128)} %rate.1, ...), custom_call_target="tpu_custom_call" | custom-call | flops 12000000000 | bytes 8000000 | tf_op jit(solution)/shard_map/layer/pallas_call | solution.py:575
  94.9 1.9 %copy.21 = bf16[1024,256]{1,0:T(8,128)(2,1)} copy(bf16[1024,256]{1,0:T(8,128)(2,1)} %layer.1) | data formatting | bytes 1048576

commit v4 on v3

--- a/solution.py
+++ b/solution.py
@@ -21,15 +21,17 @@
 QROWS = 48
 MROWS = 64
 CHUNKS = 4
-N_PUT = 176
+N_PUT = 224
 STEPS = (
-    "bA", "bB", "b0", "s1", "gy1", "gz2", "ia", "ib", "s2", "dy2", "gz3", "dz1", "s3", "gy2",
-    "gr-1", "gr0", "gr1", "gz4", "gy3", "fin0", "Ai0", "fin1", "Ai1", "fin2", "fin3", "gr2",
-    "dz2", "Ai2", "Ar0", "gr-2", "gy4", "Ar1", "Ai3", "Ar2", "Af0", "Af1", "P0", "Bi0", "dz3",
-    "P1", "Bi1", "gr3", "Ar3", "Af2", "gr-3", "P2", "Bi2", "Br0", "Br1", "dz4", "Af3", "gr4",
-    "P3", "Bi3", "Br2", "Bf0", "Bf1", "H0", "D0", "H1", "Bf2", "Br3", "D1", "E0", "C10", "E1",
-    "H2", "Bf3", "C11", "D2", "C20", "E2", "H3", "C12", "C21", "D3", "E3", "C30", "C13", "C22",
-    "C31", "C23", "C32", "C33",
+    "gz1", "spread", "dz1", "uy1", "gy0", "bA", "bB", "b0", "s1", "gz2", "gy1", "dz2", "share",
+    "s2", "uy2", "gr0", "ia", "gy2", "gz3", "ib", "gr1", "dz3", "gr-1", "u21", "gr2", "gz4", "s3",
+    "dz4", "gy3", "u31", "fin0", "Ai0", "dy1", "u11", "u01", "gy4", "fin1", "u32", "u22", "fin2",
+    "Ai2", "fin3", "u12", "Ar0", "Ai1", "Ar2", "u02", "Af0", "u33", "gr-3", "gr-2", "dy0", "Ai3",
+    "Ar1", "P0", "Bi0", "Af2", "u23", "gr4", "P2", "u13", "Bi2", "u03", "Af1", "gr3", "Ar3",
+    "u24", "Br0", "u14", "dr1", "Br2", "P1", "Af3", "u04", "Bi1", "u34", "P3", "dr0", "Bf2",
+    "Bi3", "Bf0", "H2", "Br1", "H0", "Br3", "D0", "E0", "Bf1", "D2", "C10", "E2", "H1", "C12",
+    "Bf3", "D1", "C20", "E1", "H3", "C11", "C22", "D3", "C30", "E3", "C13", "C21", "C32", "C23",
+    "C31", "C33",
 )
 
 
@@ -96,7 +98,7 @@
     raw_x, raw_g, raw_k, raw_q, raw_t, xf, gf, pad, rim_x, rim_k, rim_q, rim_t,
     ctab, cols, keys, queries, values, local, gates, upd, starts,
     msg1, buf1, msg2, buf2, msg3, enter,
-    gu, dn, wo, res, mx, st, nb, hidden, ps, pr, po, relay_l, relay_r, qs, from_l, from_r,
+    gu, dn, wo, res, rn, mx, st, nb, hidden, ps, pr, po, relay_l, relay_r, qs, from_l, from_r,
     local_sem, send_sem, recv_sem,
 ):
     sp = lax.axis_index("sp")
@@ -121,8 +123,10 @@
 
     y_peers = [{"sp": z * NY + ymod(y + j)} for j in range(1, NY)]
     z_peers = [{"sp": zmod(z + j) * NY + y} for j in range(1, NZ)]
-    up_y, down_y = {"sp": z * NY + ymod(y + 1)}, {"sp": z * NY + ymod(y - 1)}
-    up_z, down_z = {"sp": zmod(z + 1) * NY + y}, {"sp": zmod(z - 1) * NY + y}
+    to_up_y, to_down_y = {"sp": z * NY + ymod(y + 1)}, {"sp": z * NY + ymod(y - 1)}
+    to_up_z, to_down_z = {"sp": zmod(z + 1) * NY + y}, {"sp": zmod(z - 1) * NY + y}
+    odd = lax.rem(x, 2)
+    even = 1 - odd
     slot_l = lax.rem(x + NX - 1, NX) * 2 + core
     slot_r = lax.rem(x + 1, NX) * 2 + core
     slot_o = lax.rem(x + 2, NX) * 2 + core
@@ -139,7 +143,7 @@
         (k2t, raw_t.at[0:64]),
         (q2t, raw_t.at[64:128]),
         (hg, raw_g),
-        (out_w, wo),
+        (out_w, wo.at[:, 0:256]),
         (resid, res),
     ]
     own = [pltpu.make_async_copy(a, b, local_sem.at[n]) for n, (a, b) in enumerate(wanted)]
@@ -193,7 +197,7 @@
     def need(*key):
         if key not in have:
             have.add(key)
-            arrive(got[key])
+            arrive(got[key if len(key) > 1 else key[0]])
 
     tail = pl.ds(length - 16, 16)
     rims = [
@@ -206,41 +210,103 @@
     def both(ref_a, ref_b, to_a, to_b):
         return net.put(ref_a, ref_a, to_a), net.put(ref_b, ref_b, to_b)
 
-    def gu_z(r):
+    def gate_z(r):
         need("gz", r - 1)
         a, b = zmod(z - (r - 1)), zmod(z + (r - 1))
         if r == 4:
-            got["gz", r] = both(gu.at[a, y, :, 0:width], gu.at[b, y, :, width:], up_z, down_z)
+            got["gz", r] = both(
+                gu.at[a, y, 0:32, 0:width], gu.at[b, y, 32:64, 0:width], to_up_z, to_down_z)
         else:
-            got["gz", r] = both(gu.at[a, y], gu.at[b, y], up_z, down_z)
-
-    def gu_y(*ks):
+            got["gz", r] = both(
+                gu.at[a, y, :, 0:width], gu.at[b, y, :, 0:width], to_up_z, to_down_z)
+
+    def gate_y(*ks):
         for k in ks:
             need("gz", abs(k))
-            zz = zmod(z + k)
-            got["gy", k] = both(gu.at[zz, y], gu.at[zz, y], up_y, down_y)
-
-    def gu_y_relay(k):
+            ref = gu.at[zmod(z + k), y, :, 0:width]
+            got["gy", k] = both(ref, ref, to_up_y, to_down_y)
+
+    def gate_relay(k):
         arrive(got["gy", k])
         zz = zmod(z + k)
         got["gr", k] = both(
-            gu.at[zz, ymod(y - 1), :, 0:width], gu.at[zz, ymod(y + 1), :, width:], up_y, down_y)
-
-    def dn_y(r):
+            gu.at[zz, ymod(y - 1), 0:32, 0:width], gu.at[zz, ymod(y + 1), 32:64, 0:width],
+            to_up_y, to_down_y)
+
+    def up_y(r):
         if r == 1:
-            got["dy", 1] = both(dn.at[z, y], dn.at[z, y], up_y, down_y)
+            ref = gu.at[z, y, :, width:]
+            got["uy", 1] = both(ref, ref, to_up_y, to_down_y)
         else:
-            arrive(got["dy", 1])
-            got["dy", 2] = both(
-                dn.at[z, ymod(y - 1), 0:32], dn.at[z, ymod(y + 1), 32:64], up_y, down_y)
-
-    def dn_z(r):
-        arrive(got["dz", r - 1] if r > 1 else got["dy", 2])
+            need("uy", 1)
+            got["uy", 2] = both(
+                gu.at[z, ymod(y - 1), 0:32, width:], gu.at[z, ymod(y + 1), 32:64, width:],
+                to_up_y, to_down_y)
+
+    def up_z(c, r):
+        if r > 1:
+            arrive(got["uz", c, r - 1])
+        elif c > 0:
+            need("uy", 2 if c == 3 else 1)
+        col = ymod(y + (0, -1, 1, 2)[c])
         a, b = zmod(z - (r - 1)), zmod(z + (r - 1))
         if r == 4:
-            got["dz", r] = both(dn.at[a, 0:2], dn.at[b, 2:4], up_z, down_z)
+            got["uz", c, r] = both(
+                gu.at[a, col, 0:32, width:], gu.at[b, col, 32:64, width:], to_up_z, to_down_z)
         else:
-            got["dz", r] = both(dn.at[a], dn.at[b], up_z, down_z)
+            got["uz", c, r] = both(
+                gu.at[a, col, :, width:], gu.at[b, col, :, width:], to_up_z, to_down_z)
+
+    def down_z(r):
+        if r > 1:
+            arrive(got["dz", r - 1])
+        a, b = zmod(z - (r - 1)), zmod(z + (r - 1))
+        if r == 4:
+            got["dz", r] = both(dn.at[a, y, 0:32], dn.at[b, y, 32:64], to_up_z, to_down_z)
+        else:
+            got["dz", r] = both(dn.at[a, y], dn.at[b, y], to_up_z, to_down_z)
+
+    def down_y(h):
+        need("dz", 4)
+        ref = dn.at[4 * h : 4 * h + 4, y]
+        got["dy", h] = both(ref, ref, to_up_y, to_down_y)
+
+    def down_relay(h):
+        arrive(got["dy", h])
+        got["dr", h] = both(
+            dn.at[4 * h : 4 * h + 4, ymod(y - 1), 0:32], dn.at[4 * h : 4 * h + 4, ymod(y + 1), 32:64],
+            to_up_y, to_down_y)
+
+    def share():
+        own[9].wait()
+        own[10].wait()
+        got["share"] = (
+            net.put(res.at[:, even, :, 0:128], rn.at[0], x_left),
+            net.put(res.at[:, even, :, 128:256], rn.at[1], x_right),
+            net.put(wo.at[:, 0:128], wo.at[:, 256:384], x_left),
+            net.put(wo.at[:, 128:256], wo.at[:, 384:512], x_right),
+        )
+
+    def mix_first(k):
+        a, b = mx.at[k, tp, odd, 0:64], mx.at[k, tp, odd, 64:128]
+        ref = mx.at[k, tp, even]
+        got["A", k, 0] = (net.put(a, a, x_right), net.put(b, b, x_left),
+                          net.put(ref, ref, x_right), net.put(ref, ref, x_left))
+        ref = mx.at[k, tp, odd]
+        got["A", k, 1] = [net.put(ref, ref, partner)]
+
+    def mix_second(k):
+        arrive(got["A", k, 0])
+        a, b = mx.at[k, slot_l, even, 0:64], mx.at[k, slot_r, even, 64:128]
+        got["A", k, 2] = (net.put(a, a, x_right), net.put(b, b, x_left))
+        for slot in (slot_l, slot_r):
+            ref = mx.at[k, slot, odd]
+            got["A", k, 1] += [net.put(ref, ref, partner)]
+
+    def mix_third(k):
+        arrive(got["A", k, 2])
+        ref = mx.at[k, slot_o, odd]
+        got["A", k, 1] += [net.put(ref, ref, partner)]
 
     def tp_first(buf, key, k):
         ref = buf.at[k, tp]
@@ -263,19 +329,15 @@
     def tp_done(key, k):
         arrive(got[key, k, 1])
 
-    mark("start")
-    gu_z(1)
-    gu_y(0)
-    dn_y(1)
-
-    mark("spread")
-    xf[...] = raw_x[...].astype(F32)
-    for g in range(2):
-        pad[g, 8 : 8 + length] = xf[pl.ds(g, length, stride=2)]
-    pad[2, 8 : 8 + length] = raw_k[...].astype(F32)
-    pad[3, 8 : 8 + length] = raw_q[...].astype(F32)
-    for b in range(blocks):
-        pad[4, 8 + b * BLOCK : 8 + (b + 1) * BLOCK] = raw_t[:, b * BLOCK : (b + 1) * BLOCK].astype(F32).T
+    def spread():
+        xf[...] = raw_x[...].astype(F32)
+        for g in range(2):
+            pad[g, 8 : 8 + length] = xf[pl.ds(g, length, stride=2)]
+        pad[2, 8 : 8 + length] = raw_k[...].astype(F32)
+        pad[3, 8 : 8 + length] = raw_q[...].astype(F32)
+        for b in range(blocks):
+            pad[4, 8 + b * BLOCK : 8 + (b + 1) * BLOCK] = raw_t[:, b * BLOCK : (b + 1) * BLOCK].astype(F32).T
+
     second_taps = [jnp.concatenate([taps2[k, 0:1], taps2[k, 1:2]], axis=1) for k in range(CONV)]
     all_taps = [
         [head_taps[k, 0:1] for k in range(CONV)],
@@ -297,17 +359,16 @@
         at = pl.ds(pl.multiple_of(b * BLOCK, BLOCK), BLOCK)
         c = ctab[b]
         t = cols[b]
-        key_one, query_one, mix_two = conv(2, b), conv(3, b), conv(4, b)
+        key_one, mix_two = conv(2, b), conv(4, b)
         key_two = jnp.where(low, mix_two, 0.0)
-        query_two = jnp.where(low, pltpu.roll(mix_two, 64, 1), 0.0)
-        for g, (key, query) in enumerate([(key_one, query_one), (key_two, query_two)]):
+        queries[1, at] = jnp.where(low, pltpu.roll(mix_two, 64, 1), 0.0).astype(BF16)
+        for g, key in enumerate([key_one, key_two]):
             h = 2 * g
             v = conv(g, b) * halves(low, t[:, 4 + h : 5 + h], t[:, 5 + h : 6 + h])
             cum = halves(low, t[:, h : h + 1], t[:, h + 1 : h + 2])
             total = halves(low1, c[h : h + 1, 127:128], c[h + 1 : h + 2, 127:128])
             kb = key.astype(BF16)
             keys[g, at] = kb
-            queries[g, at] = query.astype(BF16)
             values[g, at] = v.astype(BF16)
             upd[g, b] = dot(kb, (v * jnp.exp(total - cum)).astype(BF16), 0, 0)
         return carry
@@ -393,6 +454,7 @@
         at = pl.ds(pl.multiple_of(b * BLOCK, BLOCK), BLOCK)
         t = cols[b]
         c = ctab[b]
+        queries[0, at] = conv(3, b).astype(BF16)
         for g in range(2):
             h = 2 * g
             qb, v = queries[g, at], values[g, at]
@@ -422,8 +484,7 @@
     tokens = BLOCK * per
 
     def finish(k):
-        if k == 0:
-            arrive(got["s3"])
+        need("s3")
         for i in range(per):
             b = k * per + i
             at = slice(b * BLOCK, (b + 1) * BLOCK)
@@ -441,32 +502,42 @@
                 s0 = jnp.sum(jnp.where(low, square, 0.0), axis=1, keepdims=True)
                 s1 = jnp.sum(jnp.where(low, 0.0, square), axis=1, keepdims=True)
                 scale = lax.rsqrt(halves(low, s0, s1) * (1.0 / HEAD) + EPSILON)
-                mx[k, tp, i * BLOCK : (i + 1) * BLOCK, g * 128 : (g + 1) * 128] = (
+                mx[k, tp, i, :, g * 128 : (g + 1) * 128] = (
                     m * scale * gain[g : g + 1]).astype(BF16)
 
     def project(k):
-        if k == 0:
-            own[9].wait()
-            own[10].wait()
+        need("share")
         tp_done("A", k)
         lhs = jnp.concatenate(
-            [mx[k, s, :, g * 128 : (g + 1) * 128] for g in range(2) for s in range(NTP)], axis=1)
-        row = dot(lhs, wo[...], 1, 0) + res[k * tokens : (k + 1) * tokens].astype(F32)
-        st[k, tp] = row.astype(BF16)
+            [mx[k, s, odd, :, g * 128 : (g + 1) * 128] for g in range(2) for s in range(NTP)], axis=1)
+        base = jnp.concatenate([res[k, odd], rn[0, k], rn[1, k]], axis=1)
+        st[k, tp] = (dot(lhs, wo[...], 1, 0) + base.astype(F32)).astype(BF16)
+
+    def stream_of(k, q, xx, cc):
+        if xx % 2 == q:
+            return st[k, 2 * xx + cc, :, 0:256]
+        return jnp.concatenate(
+            [st[k, 2 * ((xx - 1) % NX) + cc, :, 256:384], st[k, 2 * ((xx + 1) % NX) + cc, :, 384:512]],
+            axis=1)
 
     def norm_hidden(k):
         tp_done("B", k)
-        if k == 0:
-            for j in (0, 1, -1, 2, -2, 3, -3, 4):
-                arrive(got["gr", j])
-        square = jnp.zeros((tokens, 128), F32)
-        for s in range(NTP):
-            v = st[k, s].astype(F32)
-            square = square + v[:, :128] * v[:, :128] + v[:, 128:] * v[:, 128:]
-        scale = lax.rsqrt(jnp.sum(square, axis=1, keepdims=True) * (1.0 / depth) + EPSILON)
-        for s in range(NTP):
-            cut = slice(s * 256, (s + 1) * 256)
-            nb[:, cut] = (st[k, s].astype(F32) * scale * channel_gain[:, cut]).astype(BF16)
+        for j in (0, 1, -1, 2, -2, 3, -3, 4):
+            need("gr", j)
+        for c in range(NY):
+            need("uz", c, 4)
+        for q in range(2):
+            square = jnp.zeros((BLOCK, 128), F32)
+            for slot in (2 * q, 2 * q + 1, 2 * q + 4, 2 * q + 5):
+                v = st[k, slot].astype(F32)
+                for c in range(4):
+                    piece = v[:, c * 128 : (c + 1) * 128]
+                    square = square + piece * piece
+            scale = lax.rsqrt(jnp.sum(square, axis=1, keepdims=True) * (1.0 / depth) + EPSILON)
+            for slot in range(NTP):
+                cut = slice(slot * 256, (slot + 1) * 256)
+                v = stream_of(k, q, slot // 2, slot % 2).astype(F32)
+                nb[q * BLOCK : (q + 1) * BLOCK, cut] = (v * scale * channel_gain[:, cut]).astype(BF16)
         pair = dot(nb[...], gu[...].reshape(depth, 2 * width), 1, 0)
         hidden[k] = (silu(pair[:, :width]) * pair[:, width:]).astype(BF16)
 
@@ -477,8 +548,8 @@
         return dot(hidden[k], dn[d].reshape(256, width), 1, 1).astype(BF16)
 
     def down_partner(k):
-        if k == 0:
-            arrive(got["dz", 4])
+        need("dr", 0)
+        need("dr", 1)
         for j in order:
             ps[k, j] = down(k, dests[j] + 1 - core)
             got["P", k, j] = net.put(ps.at[k, j], pr.at[k, j], partner)
@@ -512,9 +583,17 @@
         total = pair_sum(k, 0)
         arrive(got["C2", k])
         total = total + from_l[k].astype(F32) + from_r[k].astype(F32)
-        out[k * tokens : (k + 1) * tokens] = (st[k, tp].astype(F32) + 0.5 * total).astype(BF16)
+        mine = st[k, tp, :, 0:256].astype(F32)
+        other = jnp.concatenate(
+            [st[k, slot_l, :, 256:384], st[k, slot_r, :, 384:512]], axis=1).astype(F32)
+        for q in range(2):
+            at = k * tokens + q * BLOCK
+            stream = jnp.where(odd == q, mine, other)
+            out[at : at + BLOCK] = (
+                stream + 0.5 * total[q * BLOCK : (q + 1) * BLOCK]).astype(BF16)
 
     run = {
+        "spread": spread,
         "bA": lambda: run_blocks(1, 5),
         "bB": lambda: run_blocks(5, 7),
         "b0": last_block,
@@ -523,18 +602,26 @@
         "s3": stage3,
         "ia": inside_a,
         "ib": inside_b,
-        "gy1": lambda: gu_y(1, -1),
-        "gy2": lambda: gu_y(2, -2),
-        "gy3": lambda: gu_y(3, -3),
-        "gy4": lambda: gu_y(4),
-        "dy2": lambda: dn_y(2),
+        "gy0": lambda: gate_y(0),
+        "gy1": lambda: gate_y(1, -1),
+        "gy2": lambda: gate_y(2, -2),
+        "gy3": lambda: gate_y(3, -3),
+        "gy4": lambda: gate_y(4),
+        "uy1": lambda: up_y(1),
+        "uy2": lambda: up_y(2),
+        "dy0": lambda: down_y(0),
+        "dy1": lambda: down_y(1),
+        "dr0": lambda: down_relay(0),
+        "dr1": lambda: down_relay(1),
+        "share": share,
     }
-    for r in (2, 3, 4):
-        run[f"gz{r}"] = functools.partial(gu_z, r)
     for r in (1, 2, 3, 4):
-        run[f"dz{r}"] = functools.partial(dn_z, r)
+        run[f"gz{r}"] = functools.partial(gate_z, r)
+        for c in range(NY):
+            run[f"u{c}{r}"] = functools.partial(up_z, c, r)
+        run[f"dz{r}"] = functools.partial(down_z, r)
     for k in (0, 1, -1, 2, -2, 3, -3, 4):
-        run[f"gr{k}"] = functools.partial(gu_y_relay, k)
+        run[f"gr{k}"] = functools.partial(gate_relay, k)
     for k in range(CHUNKS):
         run[f"fin{k}"] = functools.partial(finish, k)
         run[f"P{k}"] = functools.partial(project, k)
@@ -544,10 +631,12 @@
         run[f"C1{k}"] = functools.partial(sum_first, k)
         run[f"C2{k}"] = functools.partial(sum_second, k)
         run[f"C3{k}"] = functools.partial(sum_third, k)
-        for key, buf in (("A", mx), ("B", st)):
-            run[f"{key}i{k}"] = functools.partial(tp_first, buf, key, k)
-            run[f"{key}r{k}"] = functools.partial(tp_second, buf, key, k)
-            run[f"{key}f{k}"] = functools.partial(tp_third, buf, key, k)
+        run[f"Ai{k}"] = functools.partial(mix_first, k)
+        run[f"Ar{k}"] = functools.partial(mix_second, k)
+        run[f"Af{k}"] = functools.partial(mix_third, k)
+        run[f"Bi{k}"] = functools.partial(tp_first, st, "B", k)
+        run[f"Br{k}"] = functools.partial(tp_second, st, "B", k)
+        run[f"Bf{k}"] = functools.partial(tp_third, st, "B", k)
     for name in STEPS:
         mark(name)
         run.pop(name)()
@@ -589,8 +678,9 @@
             fl(2, blocks, 128, 128), bf(2, blocks, 128, 128),
             bf(NY, MROWS, 128), bf(NY, MROWS, 128), bf(MROWS, 128), bf(NZ, MROWS, 128),
             bf(NY, QROWS, 128), bf(NY * QROWS, 128),
-            bf(NZ, NY, 64, 2 * width), bf(NZ, NY, 64, width), bf(2048, 256), bf(length, 256),
-            bf(CHUNKS, NTP, tokens, 256), bf(CHUNKS, NTP, tokens, 256),
+            bf(NZ, NY, 64, 2 * width), bf(NZ, NY, 64, width), bf(2048, 512),
+            bf(CHUNKS, 2, BLOCK, 256), bf(2, CHUNKS, BLOCK, 128),
+            bf(CHUNKS, NTP, 2, BLOCK, 256), bf(CHUNKS, NTP, BLOCK, 512),
             bf(tokens, 2048), bf(CHUNKS, tokens, width),
             bf(CHUNKS, NX, tokens, 256), bf(CHUNKS, NX, tokens, 256), bf(CHUNKS, NX, tokens, 256),
             bf(CHUNKS, tokens // 2, 256), bf(CHUNKS, tokens // 2, 256),
@@ -646,7 +736,7 @@
             second_group_keys.T,
             second_group_queries.T,
             output_weight.reshape(-1, output_weight.shape[2]),
-            residual,
+            residual.reshape(CHUNKS, 2, BLOCK, residual.shape[1]),
             channel_gate_weight,
             channel_up_weight,
             channel_down_weight,

time: 96.9 us -> 93.1 us (0.961)
  Pallas kernels: 94.9 us -> 91.1 us
    pallas_call x1, Pallas kernels: 94.9 us -> 91.1 us  [layer(): pl.pallas_call(layer_kernel, out_shape=jax.ShapeDtypeStruct((length, 256)...]
where the time goes in v4:
time: 93.1 us; the launch traced here: 92.9 us
  Pallas kernels  91.1 us (98%)
  local copies, waits for them, and re-layouts  1.87 us (2%)
    pallas_call x1, Pallas kernels, layer(): pl.pallas_call(layer_kernel, out_shape=jax.ShapeDtypeStruct((length, 256)...  91.1 us
    unnamed x1, local copies, waits for them, and re-layouts  1.87 us

profile of v4, /device:TPU:1, one launch (start us, length us, event | category | flops | bytes accessed | tf_op | source)
XLA Modules:
  0.0 92.9 jit_solution(10929422228428694632)
XLA Ops:
  0.0 91.1 %layer.1 = bf16[1024,256]{1,0:T(8,128)(2,1)} custom-call(f32[2,2,1024]{2,1,0:T(2,128)} %bitcast.15, f32[2,2,1024]{2,1,0:T(2,128)} %bitcast.16, f32[4,2,128]{2,1,0:T(2,128)} %head_taps.1, f32[4,2,128]{2,1,0:T(2,128)} %taps1.1, f32[4,2,64]{2,1,0:T(2,128)} %taps2.1, f32[2,128]{1,0:T(2,128)} %gain.1, f32[1,2048]{1,0:T(1,128)} %bitcast.17, f32[2,2]{1,0:T(2,128)} %rate.1, ...), custom_call_target="tpu_custom_call" | custom-call | flops 12000000000 | bytes 8000000 | tf_op jit(solution)/shard_map/layer/pallas_call | solution.py:664
  91.1 1.9 %copy.21 = bf16[1024,256]{1,0:T(8,128)(2,1)} copy(bf16[1024,256]{1,0:T(8,128)(2,1)} %layer.1) | data formatting | bytes 1048576

commit v5 on v4

--- a/solution.py
+++ b/solution.py
@@ -21,17 +21,18 @@
 QROWS = 48
 MROWS = 64
 CHUNKS = 4
-N_PUT = 224
+N_PUT = 236
+SPLIT = 512
 STEPS = (
-    "gz1", "spread", "dz1", "uy1", "gy0", "bA", "bB", "b0", "s1", "gz2", "gy1", "dz2", "share",
-    "s2", "uy2", "gr0", "ia", "gy2", "gz3", "ib", "gr1", "dz3", "gr-1", "u21", "gr2", "gz4", "s3",
-    "dz4", "gy3", "u31", "fin0", "Ai0", "dy1", "u11", "u01", "gy4", "fin1", "u32", "u22", "fin2",
-    "Ai2", "fin3", "u12", "Ar0", "Ai1", "Ar2", "u02", "Af0", "u33", "gr-3", "gr-2", "dy0", "Ai3",
-    "Ar1", "P0", "Bi0", "Af2", "u23", "gr4", "P2", "u13", "Bi2", "u03", "Af1", "gr3", "Ar3",
-    "u24", "Br0", "u14", "dr1", "Br2", "P1", "Af3", "u04", "Bi1", "u34", "P3", "dr0", "Bf2",
-    "Bi3", "Bf0", "H2", "Br1", "H0", "Br3", "D0", "E0", "Bf1", "D2", "C10", "E2", "H1", "C12",
-    "Bf3", "D1", "C20", "E1", "H3", "C11", "C22", "D3", "C30", "E3", "C13", "C21", "C32", "C23",
-    "C31", "C33",
+    "gz1", "ey1", "dz1", "spread", "gy0", "uy1", "u01", "bA", "bB", "b0", "share", "gz2", "s1",
+    "dz2", "ey2", "gr0", "gy1", "s2", "ia", "dz3", "gz3", "ez1", "uy2", "gy2", "gr1", "u21", "ib",
+    "dz4", "u02", "s3", "gr-1", "u11", "gy3", "fin0", "Ai0", "fin1", "fin2", "dy1", "gr-2", "u22",
+    "fin3", "gr2", "u31", "dy0", "Ai1", "Ar0", "Ai2", "gr3", "gz4", "gr-3", "u12", "Ar1", "u03",
+    "Ai3", "ez2", "Af0", "P0", "Ar2", "u32", "Bi0", "gy4", "Af1", "u23", "P1", "Af2", "Bi1",
+    "Ar3", "dr1", "u13", "u33", "Br0", "u24", "P2", "Br1", "u14", "Bi2", "ez3", "u04", "Af3",
+    "gr4", "P3", "dr0", "u34", "Bi3", "Bf0", "Bf1", "ez4", "N0", "N1", "Br2", "H1", "D1", "Br3",
+    "H0", "Bf2", "D0", "E1", "C11", "N2", "E0", "Bf3", "C10", "H2", "D2", "C21", "N3", "E2",
+    "C12", "H3", "C20", "D3", "C31", "E3", "C13", "C22", "C30", "C23", "C32", "C33",
 )
 
 
@@ -262,20 +263,46 @@
             arrive(got["dz", r - 1])
         a, b = zmod(z - (r - 1)), zmod(z + (r - 1))
         if r == 4:
-            got["dz", r] = both(dn.at[a, y, 0:32], dn.at[b, y, 32:64], to_up_z, to_down_z)
+            got["dz", r] = both(
+                dn.at[a, y, 0:32, 0:SPLIT], dn.at[b, y, 32:64, 0:SPLIT], to_up_z, to_down_z)
         else:
-            got["dz", r] = both(dn.at[a, y], dn.at[b, y], to_up_z, to_down_z)
+            got["dz", r] = both(
+                dn.at[a, y, :, 0:SPLIT], dn.at[b, y, :, 0:SPLIT], to_up_z, to_down_z)
 
     def down_y(h):
         need("dz", 4)
-        ref = dn.at[4 * h : 4 * h + 4, y]
+        ref = dn.at[4 * h : 4 * h + 4, y, :, 0:SPLIT]
         got["dy", h] = both(ref, ref, to_up_y, to_down_y)
 
     def down_relay(h):
         arrive(got["dy", h])
+        part = pl.ds(4 * h, 4)
         got["dr", h] = both(
-            dn.at[4 * h : 4 * h + 4, ymod(y - 1), 0:32], dn.at[4 * h : 4 * h + 4, ymod(y + 1), 32:64],
+            dn.at[part, ymod(y - 1), 0:32, 0:SPLIT], dn.at[part, ymod(y + 1), 32:64, 0:SPLIT],
             to_up_y, to_down_y)
+
+    def rest_y(r):
+        if r == 1:
+            ref = dn.at[z, y, :, SPLIT:]
+            got["ey", 1] = both(ref, ref, to_up_y, to_down_y)
+        else:
+            need("ey", 1)
+            got["ey", 2] = both(
+                dn.at[z, ymod(y - 1), 0:32, SPLIT:], dn.at[z, ymod(y + 1), 32:64, SPLIT:],
+                to_up_y, to_down_y)
+
+    def rest_z(r):
+        if r == 1:
+            need("ey", 2)
+        else:
+            arrive(got["ez", r - 1])
+        a, b = zmod(z - (r - 1)), zmod(z + (r - 1))
+        if r == 4:
+            got["ez", r] = both(
+                dn.at[a, 0:2, :, SPLIT:], dn.at[b, 2:4, :, SPLIT:], to_up_z, to_down_z)
+        else:
+            got["ez", r] = both(
+                dn.at[a, :, :, SPLIT:], dn.at[b, :, :, SPLIT:], to_up_z, to_down_z)
 
     def share():
         own[9].wait()
@@ -520,12 +547,8 @@
             [st[k, 2 * ((xx - 1) % NX) + cc, :, 256:384], st[k, 2 * ((xx + 1) % NX) + cc, :, 384:512]],
             axis=1)
 
-    def norm_hidden(k):
+    def norm(k):
         tp_done("B", k)
-        for j in (0, 1, -1, 2, -2, 3, -3, 4):
-            need("gr", j)
-        for c in range(NY):
-            need("uz", c, 4)
         for q in range(2):
             square = jnp.zeros((BLOCK, 128), F32)
             for slot in (2 * q, 2 * q + 1, 2 * q + 4, 2 * q + 5):
@@ -537,8 +560,14 @@
             for slot in range(NTP):
                 cut = slice(slot * 256, (slot + 1) * 256)
                 v = stream_of(k, q, slot // 2, slot % 2).astype(F32)
-                nb[q * BLOCK : (q + 1) * BLOCK, cut] = (v * scale * channel_gain[:, cut]).astype(BF16)
-        pair = dot(nb[...], gu[...].reshape(depth, 2 * width), 1, 0)
+                nb[k, q * BLOCK : (q + 1) * BLOCK, cut] = (v * scale * channel_gain[:, cut]).astype(BF16)
+
+    def hidden_units(k):
+        for j in (0, 1, -1, 2, -2, 3, -3, 4):
+            need("gr", j)
+        for c in range(NY):
+            need("uz", c, 4)
+        pair = dot(nb[k], gu[...].reshape(depth, 2 * width), 1, 0)
         hidden[k] = (silu(pair[:, :width]) * pair[:, width:]).astype(BF16)
 
     order = (2, 3, 1, 0)
@@ -550,8 +579,10 @@
     def down_partner(k):
         need("dr", 0)
         need("dr", 1)
+        need("ez", 4)
         for j in order:
             ps[k, j] = down(k, dests[j] + 1 - core)
+        for j in order:
             got["P", k, j] = net.put(ps.at[k, j], pr.at[k, j], partner)
 
     def down_own(k):
@@ -611,6 +642,8 @@
         "uy2": lambda: up_y(2),
         "dy0": lambda: down_y(0),
         "dy1": lambda: down_y(1),
+        "ey1": lambda: rest_y(1),
+        "ey2": lambda: rest_y(2),
         "dr0": lambda: down_relay(0),
         "dr1": lambda: down_relay(1),
         "share": share,
@@ -620,12 +653,14 @@
         for c in range(NY):
             run[f"u{c}{r}"] = functools.partial(up_z, c, r)
         run[f"dz{r}"] = functools.partial(down_z, r)
+        run[f"ez{r}"] = functools.partial(rest_z, r)
     for k in (0, 1, -1, 2, -2, 3, -3, 4):
         run[f"gr{k}"] = functools.partial(gate_relay, k)
     for k in range(CHUNKS):
         run[f"fin{k}"] = functools.partial(finish, k)
         run[f"P{k}"] = functools.partial(project, k)
-        run[f"H{k}"] = functools.partial(norm_hidden, k)
+        run[f"N{k}"] = functools.partial(norm, k)
+        run[f"H{k}"] = functools.partial(hidden_units, k)
         run[f"D{k}"] = functools.partial(down_partner, k)
         run[f"E{k}"] = functools.partial(down_own, k)
         run[f"C1{k}"] = functools.partial(sum_first, k)
@@ -681,7 +716,7 @@
             bf(NZ, NY, 64, 2 * width), bf(NZ, NY, 64, width), bf(2048, 512),
             bf(CHUNKS, 2, BLOCK, 256), bf(2, CHUNKS, BLOCK, 128),
             bf(CHUNKS, NTP, 2, BLOCK, 256), bf(CHUNKS, NTP, BLOCK, 512),
-            bf(tokens, 2048), bf(CHUNKS, tokens, width),
+            bf(CHUNKS, tokens, 2048), bf(CHUNKS, tokens, width),
             bf(CHUNKS, NX, tokens, 256), bf(CHUNKS, NX, tokens, 256), bf(CHUNKS, NX, tokens, 256),
             bf(CHUNKS, tokens // 2, 256), bf(CHUNKS, tokens // 2, 256),
             bf(CHUNKS, NX, tokens, 256), bf(CHUNKS, tokens, 256), bf(CHUNKS, tokens, 256),

time: 93.1 us -> 91.7 us (0.985)
  Pallas kernels: 91.1 us -> 89.6 us
    pallas_call x1, Pallas kernels: 91.1 us -> 89.6 us  [layer(): pl.pallas_call(layer_kernel, out_shape=jax.ShapeDtypeStruct((length, 256)...]
where the time goes in v5:
time: 91.7 us; the launch traced here: 91.5 us
  Pallas kernels  89.6 us (98%)
  local copies, waits for them, and re-layouts  1.87 us (2%)
    pallas_call x1, Pallas kernels, layer(): pl.pallas_call(layer_kernel, out_shape=jax.ShapeDtypeStruct((length, 256)...  89.6 us
    unnamed x1, local copies, waits for them, and re-layouts  1.87 us

profile of v5, /device:TPU:1, one launch (start us, length us, event | category | flops | bytes accessed | tf_op | source)
XLA Modules:
  0.0 91.5 jit_solution(12312251854477298765)
XLA Ops:
  0.0 89.6 %layer.1 = bf16[1024,256]{1,0:T(8,128)(2,1)} custom-call(f32[2,2,1024]{2,1,0:T(2,128)} %bitcast.15, f32[2,2,1024]{2,1,0:T(2,128)} %bitcast.16, f32[4,2,128]{2,1,0:T(2,128)} %head_taps.1, f32[4,2,128]{2,1,0:T(2,128)} %taps1.1, f32[4,2,64]{2,1,0:T(2,128)} %taps2.1, f32[2,128]{1,0:T(2,128)} %gain.1, f32[1,2048]{1,0:T(1,128)} %bitcast.17, f32[2,2]{1,0:T(2,128)} %rate.1, ...), custom_call_target="tpu_custom_call" | custom-call | flops 12000000000 | bytes 8000000 | tf_op jit(solution)/shard_map/layer/pallas_call | solution.py:699
  89.6 1.9 %copy.21 = bf16[1024,256]{1,0:T(8,128)(2,1)} copy(bf16[1024,256]{1,0:T(8,128)(2,1)} %layer.1) | data formatting | bytes 1048576

commit v6 on v5

--- a/solution.py
+++ b/solution.py
@@ -24,15 +24,15 @@
 N_PUT = 236
 SPLIT = 512
 STEPS = (
-    "gz1", "ey1", "dz1", "spread", "gy0", "uy1", "u01", "bA", "bB", "b0", "share", "gz2", "s1",
-    "dz2", "ey2", "gr0", "gy1", "s2", "ia", "dz3", "gz3", "ez1", "uy2", "gy2", "gr1", "u21", "ib",
-    "dz4", "u02", "s3", "gr-1", "u11", "gy3", "fin0", "Ai0", "fin1", "fin2", "dy1", "gr-2", "u22",
-    "fin3", "gr2", "u31", "dy0", "Ai1", "Ar0", "Ai2", "gr3", "gz4", "gr-3", "u12", "Ar1", "u03",
-    "Ai3", "ez2", "Af0", "P0", "Ar2", "u32", "Bi0", "gy4", "Af1", "u23", "P1", "Af2", "Bi1",
-    "Ar3", "dr1", "u13", "u33", "Br0", "u24", "P2", "Br1", "u14", "Bi2", "ez3", "u04", "Af3",
-    "gr4", "P3", "dr0", "u34", "Bi3", "Bf0", "Bf1", "ez4", "N0", "N1", "Br2", "H1", "D1", "Br3",
-    "H0", "Bf2", "D0", "E1", "C11", "N2", "E0", "Bf3", "C10", "H2", "D2", "C21", "N3", "E2",
-    "C12", "H3", "C20", "D3", "C31", "E3", "C13", "C22", "C30", "C23", "C32", "C33",
+    "gz1", "ey1", "dz1", "spread", "tables", "gy0", "uy1", "u01", "bA", "bB", "b0", "share",
+    "gz2", "s1", "dz2", "ey2", "gr0", "gy1", "s2", "ia", "dz3", "gz3", "ez1", "uy2", "gy2", "gr1",
+    "u21", "ib", "dz4", "u02", "s3", "gr-1", "u11", "gy3", "fin0", "Ai0", "fin1", "fin2", "dy1",
+    "gr-2", "u22", "fin3", "gr2", "u31", "dy0", "Ai1", "Ar0", "Ai2", "gr3", "gz4", "gr-3", "u12",
+    "Ar1", "u03", "Ai3", "ez2", "Af0", "P0", "Ar2", "u32", "Bi0", "gy4", "Af1", "u23", "P1",
+    "Af2", "Bi1", "Ar3", "dr1", "u13", "u33", "Br0", "u24", "P2", "Br1", "u14", "Bi2", "ez3",
+    "u04", "Af3", "gr4", "P3", "dr0", "u34", "Bi3", "Bf0", "Bf1", "ez4", "N0", "N1", "Br2", "H1",
+    "D1", "Br3", "H0", "Bf2", "D0", "E1", "C11", "N2", "E0", "Bf3", "C10", "H2", "D2", "C21",
+    "N3", "E2", "C12", "H3", "C20", "D3", "C31", "E3", "C13", "C22", "C30", "C23", "C32", "C33",
 )
 
 
@@ -93,9 +93,10 @@
 
 
 def layer_kernel(
-    step_in, extra, head_taps, taps1, taps2, gain, channel_gain, rate,
+    hbm_step, hbm_extra, hbm_head, hbm_taps1, hbm_taps2, hbm_gain, hbm_channel, hbm_rate,
     hx, hg, k1, q1, k2t, q2t, out_w, resid, gate_w, up_w, down_w,
-    out,
+    hbm_out,
+    step_in, extra, head_taps, taps1, taps2, gain, channel_gain, rate, out,
     raw_x, raw_g, raw_k, raw_q, raw_t, xf, gf, pad, rim_x, rim_k, rim_q, rim_t,
     ctab, cols, keys, queries, values, local, gates, upd, starts,
     msg1, buf1, msg2, buf2, msg3, enter,
@@ -146,17 +147,24 @@
         (hg, raw_g),
         (out_w, wo.at[:, 0:256]),
         (resid, res),
+        (hbm_step, step_in),
+        (hbm_extra, extra),
+        (hbm_rate, rate),
+        (hbm_head, head_taps),
+        (hbm_taps1, taps1),
+        (hbm_taps2, taps2),
+        (hbm_gain, gain),
+        (hbm_channel, channel_gain),
     ]
-    own = [pltpu.make_async_copy(a, b, local_sem.at[n]) for n, (a, b) in enumerate(wanted)]
-    for copy in own:
-        copy.start()
-
     barrier = pltpu.get_barrier_semaphore()
     greet = [{"sp": right}, {"sp": left}] + y_peers + z_peers + [partner, x_right, x_left]
     for peer in greet:
         pl.semaphore_signal(barrier, inc=1, device_id=peer, device_id_type=MESH)
 
-    mark("tables")
+    own = [pltpu.make_async_copy(a, b, local_sem.at[n]) for n, (a, b) in enumerate(wanted)]
+    for copy in own:
+        copy.start()
+
     row8 = lax.broadcasted_iota(jnp.int32, (8, 128), 0)
     low = lax.broadcasted_iota(jnp.int32, (BLOCK, 128), 1) < HEAD
     low1 = lax.broadcasted_iota(jnp.int32, (1, 128), 1) < HEAD
@@ -164,27 +172,6 @@
     at_col = lax.broadcasted_iota(jnp.int32, (BLOCK, BLOCK), 1)
     causal = at_row >= at_col
     upper = jnp.where(at_row <= at_col, 1.0, 0.0).astype(BF16)
-    first_head = lax.broadcasted_iota(jnp.int32, (2, length), 0) == 0
-    steps = [jax.nn.softplus(step_in[g]) for g in range(2)]
-    logs = [extra[g] - steps[g] * jnp.where(first_head, rate[g, 0], rate[g, 1]) for g in range(2)]
-    table = jnp.concatenate(
-        [v[:, b * BLOCK : (b + 1) * BLOCK] for b in range(blocks) for v in logs + steps], axis=0)
-    rows = table.shape[0]
-    sums = dot(jnp.concatenate(split_three(table), axis=0), upper, 1, 0)
-    sums = sums[0:rows] + sums[rows : 2 * rows] + sums[2 * rows :]
-    offs = jnp.zeros((8, 1), F32)
-    for b in range(blocks):
-        cut = slice(8 * b, 8 * b + 8)
-        c8 = jnp.where(row8 < 4, sums[cut], table[cut])
-        ctab[b] = c8
-        e8 = jnp.exp(jnp.where(row8 < 4, c8 + offs, 0.0))
-        cols[b] = jnp.concatenate([c8, e8], axis=0).T
-        offs = offs + c8[:, 127:128]
-    log0 = halves(low1, offs[0:1], offs[1:2])
-    log1 = halves(low1, offs[2:3], offs[3:4])
-    my_logs = log_rows(log0, log1)
-    for q in range(NY):
-        msg1[q, QROWS:MROWS] = my_logs
 
     mark("barwait")
     for copy in own[:8]:
@@ -356,6 +343,31 @@
     def tp_done(key, k):
         arrive(got[key, k, 1])
 
+    def tables():
+        for copy in own[11:]:
+            copy.wait()
+        first_head = lax.broadcasted_iota(jnp.int32, (2, length), 0) == 0
+        steps = [jax.nn.softplus(step_in[g]) for g in range(2)]
+        logs = [extra[g] - steps[g] * jnp.where(first_head, rate[g : g + 1, 0:1], rate[g : g + 1, 1:2]) for g in range(2)]
+        table = jnp.concatenate(
+            [v[:, b * BLOCK : (b + 1) * BLOCK] for b in range(blocks) for v in logs + steps], axis=0)
+        rows = table.shape[0]
+        sums = dot(jnp.concatenate(split_three(table), axis=0), upper, 1, 0)
+        sums = sums[0:rows] + sums[rows : 2 * rows] + sums[2 * rows :]
+        offs = jnp.zeros((8, 1), F32)
+        for b in range(blocks):
+            cut = slice(8 * b, 8 * b + 8)
+            c8 = jnp.where(row8 < 4, sums[cut], table[cut])
+            ctab[b] = c8
+            e8 = jnp.exp(jnp.where(row8 < 4, c8 + offs, 0.0))
+            cols[b] = jnp.concatenate([c8, e8], axis=0).T
+            offs = offs + c8[:, 127:128]
+        log0 = halves(low1, offs[0:1], offs[1:2])
+        log1 = halves(low1, offs[2:3], offs[3:4])
+        my_logs = log_rows(log0, log1)
+        for q in range(NY):
+            msg1[q, QROWS:MROWS] = my_logs
+
     def spread():
         xf[...] = raw_x[...].astype(F32)
         for g in range(2):
@@ -365,18 +377,14 @@
         for b in range(blocks):
             pad[4, 8 + b * BLOCK : 8 + (b + 1) * BLOCK] = raw_t[:, b * BLOCK : (b + 1) * BLOCK].astype(F32).T
 
-    second_taps = [jnp.concatenate([taps2[k, 0:1], taps2[k, 1:2]], axis=1) for k in range(CONV)]
-    all_taps = [
-        [head_taps[k, 0:1] for k in range(CONV)],
-        [head_taps[k, 1:2] for k in range(CONV)],
-        [taps1[k, 0:1] for k in range(CONV)],
-        [taps1[k, 1:2] for k in range(CONV)],
-        second_taps,
-    ]
-
     def conv(n, b):
         full = pad[n, pl.ds(pl.multiple_of(b * BLOCK, BLOCK), BLOCK + 8)]
-        taps = all_taps[n]
+        if n < 2:
+            taps = [head_taps[k, n : n + 1] for k in range(CONV)]
+        elif n < 4:
+            taps = [taps1[k, n - 2 : n - 1] for k in range(CONV)]
+        else:
+            taps = [jnp.concatenate([taps2[k, 0:1], taps2[k, 1:2]], axis=1) for k in range(CONV)]
         total = taps[0] * full[5 : 5 + BLOCK]
         for k in range(1, CONV):
             total = total + taps[k] * full[5 + k : 5 + k + BLOCK]
@@ -594,6 +602,7 @@
         return po[k, j].astype(F32) + pr[k, j].astype(F32)
 
     mid = tokens // 2
+    outs = []
 
     def sum_first(k):
         qs[k, 2] = pair_sum(k, 2).astype(BF16)
@@ -622,8 +631,13 @@
             stream = jnp.where(odd == q, mine, other)
             out[at : at + BLOCK] = (
                 stream + 0.5 * total[q * BLOCK : (q + 1) * BLOCK]).astype(BF16)
+        rows = pl.ds(k * tokens, tokens)
+        copy = pltpu.make_async_copy(out.at[rows], hbm_out.at[rows], local_sem.at[19 + k])
+        copy.start()
+        outs.append(copy)
 
     run = {
+        "tables": tables,
         "spread": spread,
         "bA": lambda: run_blocks(1, 5),
         "bB": lambda: run_blocks(5, 7),
@@ -678,16 +692,18 @@
     assert not run
 
     mark("sends")
+    for copy in outs:
+        copy.wait()
     for copy in net.sent:
         copy.wait_send()
 
 
-def layer(vmem_args, smem_arg, hbm_args):
+def layer(small_args, hbm_args):
     length = hbm_args[2].shape[0]
     blocks = length // BLOCK
     tokens = length // CHUNKS
     width = hbm_args[8].shape[1]
-    vmem = pl.BlockSpec(memory_space=pltpu.VMEM)
+    hbm = pl.BlockSpec(memory_space=pl.ANY)
     dma = pltpu.SemaphoreType.DMA
 
     def bf(*shape):
@@ -699,11 +715,11 @@
     return pl.pallas_call(
         layer_kernel,
         out_shape=jax.ShapeDtypeStruct((length, 256), BF16),
-        in_specs=[vmem] * len(vmem_args)
-        + [pl.BlockSpec(memory_space=pltpu.SMEM)]
-        + [pl.BlockSpec(memory_space=pl.ANY)] * len(hbm_args),
-        out_specs=vmem,
-        scratch_shapes=[
+        in_specs=[hbm] * (len(small_args) + len(hbm_args)),
+        out_specs=hbm,
+        scratch_shapes=[fl(*a.shape) for a in small_args]
+        + [
+            bf(length, 256),
             bf(2 * length, 128), bf(2 * length, 128), bf(length, 128), bf(length, 128),
             bf(128, length), fl(2 * length, 128), fl(2 * length, 128), fl(5, length + 8, 128),
             bf(16, 128), bf(16, 128), bf(16, 128), bf(128, 128),
@@ -720,14 +736,14 @@
             bf(CHUNKS, NX, tokens, 256), bf(CHUNKS, NX, tokens, 256), bf(CHUNKS, NX, tokens, 256),
             bf(CHUNKS, tokens // 2, 256), bf(CHUNKS, tokens // 2, 256),
             bf(CHUNKS, NX, tokens, 256), bf(CHUNKS, tokens, 256), bf(CHUNKS, tokens, 256),
-            dma((11,)), dma((N_PUT,)), dma((N_PUT,)),
+            dma((19 + CHUNKS,)), dma((N_PUT,)), dma((N_PUT,)),
         ],
         compiler_params=pltpu.CompilerParams(
             collective_id=0, has_side_effects=True, vmem_limit_bytes=58 * 1024 * 1024),
         cost_estimate=pl.CostEstimate(
             flops=12_000_000_000, bytes_accessed=8_000_000, transcendentals=4_000_000),
         name="layer",
-    )(*vmem_args, smem_arg, *hbm_args)
+    )(*small_args, *hbm_args)
 
 
 def shards(
@@ -761,8 +777,8 @@
             second_group_filter,
             head_norm_gain,
             channel_norm_gain[None],
+            head_decay_rate,
         ),
-        head_decay_rate,
         (
             grouped_head_inputs.reshape(2 * length, 128),
             head_gate_inputs.reshape(2 * length, 128),

time: 91.7 us -> 90.4 us (0.986)
  Pallas kernels: 89.6 us -> 88.4 us
    pallas_call x1, Pallas kernels: 89.6 us -> 88.4 us  [layer(): pl.pallas_call(layer_kernel, out_shape=jax.ShapeDtypeStruct((length, 256)...]
where the time goes in v6:
time: 90.4 us; the launch traced here: 90.3 us
  Pallas kernels  88.4 us (98%)
  local copies, waits for them, and re-layouts  1.87 us (2%)
    pallas_call x1, Pallas kernels, layer(): pl.pallas_call(layer_kernel, out_shape=jax.ShapeDtypeStruct((length, 256)...  88.4 us
    unnamed x1, local copies, waits for them, and re-layouts  1.87 us

profile of v6, /device:TPU:1, one launch (start us, length us, event | category | flops | bytes accessed | tf_op | source)
XLA Modules:
  0.0 90.3 jit_solution(6804142057568541718)
XLA Ops:
  0.0 88.4 %layer.1 = bf16[1024,256]{1,0:T(8,128)(2,1)} custom-call(f32[2,2,1024]{2,1,0:T(2,128)} %bitcast.15, f32[2,2,1024]{2,1,0:T(2,128)} %bitcast.16, f32[4,2,128]{2,1,0:T(2,128)} %hbm_head.1, f32[4,2,128]{2,1,0:T(2,128)} %hbm_taps1.1, f32[4,2,64]{2,1,0:T(2,128)} %hbm_taps2.1, f32[2,128]{1,0:T(2,128)} %hbm_gain.1, f32[1,2048]{1,0:T(1,128)} %bitcast.17, ...), custom_call_target="tpu_custom_call" | custom-call | flops 12000000000 | bytes 8000000 | tf_op jit(solution)/shard_map/layer/pallas_call | solution.py:715
  88.4 1.9 %copy.21 = bf16[1024,256]{1,0:T(8,128)(2,1)} copy(bf16[1024,256]{1,0:T(8,128)(2,1)} %layer.1) | data formatting | bytes 1048576

commit v7 on v6

--- a/solution.py
+++ b/solution.py
@@ -24,15 +24,15 @@
 N_PUT = 236
 SPLIT = 512
 STEPS = (
-    "gz1", "ey1", "dz1", "spread", "tables", "gy0", "uy1", "u01", "bA", "bB", "b0", "share",
-    "gz2", "s1", "dz2", "ey2", "gr0", "gy1", "s2", "ia", "dz3", "gz3", "ez1", "uy2", "gy2", "gr1",
-    "u21", "ib", "dz4", "u02", "s3", "gr-1", "u11", "gy3", "fin0", "Ai0", "fin1", "fin2", "dy1",
-    "gr-2", "u22", "fin3", "gr2", "u31", "dy0", "Ai1", "Ar0", "Ai2", "gr3", "gz4", "gr-3", "u12",
-    "Ar1", "u03", "Ai3", "ez2", "Af0", "P0", "Ar2", "u32", "Bi0", "gy4", "Af1", "u23", "P1",
-    "Af2", "Bi1", "Ar3", "dr1", "u13", "u33", "Br0", "u24", "P2", "Br1", "u14", "Bi2", "ez3",
-    "u04", "Af3", "gr4", "P3", "dr0", "u34", "Bi3", "Bf0", "Bf1", "ez4", "N0", "N1", "Br2", "H1",
-    "D1", "Br3", "H0", "Bf2", "D0", "E1", "C11", "N2", "E0", "Bf3", "C10", "H2", "D2", "C21",
-    "N3", "E2", "C12", "H3", "C20", "D3", "C31", "E3", "C13", "C22", "C30", "C23", "C32", "C33",
+    "dz1", "spread", "gy0", "gz1", "tables", "u01", "uy1", "bA", "bB", "b0", "dz2", "s1", "share",
+    "ey1", "gz2", "gy1", "gr0", "s2", "uy2", "ey2", "ia", "gz3", "gy2", "gr1", "dz3", "ib", "u21",
+    "gz4", "s3", "gy3", "gr-1", "u11", "ez1", "dz4", "u22", "u31", "fin0", "Ai0", "fin1", "fin2",
+    "fin3", "Ai2", "gr3", "gy4", "ez2", "gr2", "u02", "dy0", "dy1", "Ar0", "u12", "Ai1", "u32",
+    "Ar2", "gr-2", "Af0", "Ai3", "gr-3", "P0", "Ar1", "Af2", "Bi0", "u23", "P2", "u13", "ez3",
+    "Bi2", "dr0", "Af1", "u33", "Br0", "u03", "gr4", "u24", "Ar3", "P1", "Br2", "dr1", "Bi1",
+    "u14", "u34", "Bf0", "Af3", "u04", "P3", "N0", "ez4", "Bf2", "Bi3", "N2", "Br1", "H0", "D0",
+    "H2", "Br3", "E0", "Bf1", "C10", "D2", "E2", "N1", "H1", "C12", "Bf3", "D1", "C20", "E1",
+    "N3", "H3", "C11", "C22", "D3", "E3", "C30", "C13", "C21", "C32", "C23", "C31", "C33",
 )
 
 
@@ -369,7 +369,7 @@
             msg1[q, QROWS:MROWS] = my_logs
 
     def spread():
-        xf[...] = raw_x[...].astype(F32)
+        xf[0 : 2 * length] = raw_x[...].astype(F32)
         for g in range(2):
             pad[g, 8 : 8 + length] = xf[pl.ds(g, length, stride=2)]
         pad[2, 8 : 8 + length] = raw_k[...].astype(F32)
@@ -507,7 +507,7 @@
 
     def inside_a():
         own[8].wait()
-        gf[...] = raw_g[...].astype(F32)
+        gf[0 : 2 * length] = raw_g[...].astype(F32)
         for g in range(2):
             gates[g] = silu(gf[pl.ds(g, length, stride=2)])
         lax.fori_loop(0, blocks // 2, inside, 0, unroll=2)
@@ -721,7 +721,7 @@
         + [
             bf(length, 256),
             bf(2 * length, 128), bf(2 * length, 128), bf(length, 128), bf(length, 128),
-            bf(128, length), fl(2 * length, 128), fl(2 * length, 128), fl(5, length + 8, 128),
+            bf(128, length), fl(2 * length + 16, 128), fl(2 * length + 16, 128), fl(5, length + 8, 128),
             bf(16, 128), bf(16, 128), bf(16, 128), bf(128, 128),
             fl(blocks, 8, 128), fl(blocks, BLOCK, 16),
             bf(2, length, 128), bf(2, length, 128), bf(2, length, 128),

time: 90.4 us -> 91.3 us (level)
  no operation moved by 1% of the time
where the time goes in v7:
time: 91.3 us; the launch traced here: 91.1 us
  Pallas kernels  89.3 us (98%)
  local copies, waits for them, and re-layouts  1.87 us (2%)
    pallas_call x1, Pallas kernels, layer(): pl.pallas_call(layer_kernel, out_shape=jax.ShapeDtypeStruct((length, 256)...  89.3 us
    unnamed x1, local copies, waits for them, and re-layouts  1.87 us

profile of v7, /device:TPU:1, one launch (start us, length us, event | category | flops | bytes accessed | tf_op | source)
XLA Modules:
  0.0 91.1 jit_solution(678444999363101829)
XLA Ops:
  0.0 89.3 %layer.1 = bf16[1024,256]{1,0:T(8,128)(2,1)} custom-call(f32[2,2,1024]{2,1,0:T(2,128)} %bitcast.15, f32[2,2,1024]{2,1,0:T(2,128)} %bitcast.16, f32[4,2,128]{2,1,0:T(2,128)} %hbm_head.1, f32[4,2,128]{2,1,0:T(2,128)} %hbm_taps1.1, f32[4,2,64]{2,1,0:T(2,128)} %hbm_taps2.1, f32[2,128]{1,0:T(2,128)} %hbm_gain.1, f32[1,2048]{1,0:T(1,128)} %bitcast.17, ...), custom_call_target="tpu_custom_call" | custom-call | flops 12000000000 | bytes 8000000 | tf_op jit(solution)/shard_map/layer/pallas_call | solution.py:715
  89.3 1.9 %copy.21 = bf16[1024,256]{1,0:T(8,128)(2,1)} copy(bf16[1024,256]{1,0:T(8,128)(2,1)} %layer.1) | data formatting | bytes 1048576

commit v8 on v6

--- a/solution.py
+++ b/solution.py
@@ -369,7 +369,7 @@
             msg1[q, QROWS:MROWS] = my_logs
 
     def spread():
-        xf[...] = raw_x[...].astype(F32)
+        xf[0 : 2 * length] = raw_x[...].astype(F32)
         for g in range(2):
             pad[g, 8 : 8 + length] = xf[pl.ds(g, length, stride=2)]
         pad[2, 8 : 8 + length] = raw_k[...].astype(F32)
@@ -507,7 +507,7 @@
 
     def inside_a():
         own[8].wait()
-        gf[...] = raw_g[...].astype(F32)
+        gf[0 : 2 * length] = raw_g[...].astype(F32)
         for g in range(2):
             gates[g] = silu(gf[pl.ds(g, length, stride=2)])
         lax.fori_loop(0, blocks // 2, inside, 0, unroll=2)
@@ -721,7 +721,7 @@
         + [
             bf(length, 256),
             bf(2 * length, 128), bf(2 * length, 128), bf(length, 128), bf(length, 128),
-            bf(128, length), fl(2 * length, 128), fl(2 * length, 128), fl(5, length + 8, 128),
+            bf(128, length), fl(2 * length + 16, 128), fl(2 * length + 16, 128), fl(5, length + 8, 128),
             bf(16, 128), bf(16, 128), bf(16, 128), bf(128, 128),
             fl(blocks, 8, 128), fl(blocks, BLOCK, 16),
             bf(2, length, 128), bf(2, length, 128), bf(2, length, 128),

time: 90.4 us -> 90.4 us (level)
  no operation moved by 1% of the time
where the time goes in v8:
time: 90.4 us; the launch traced here: 90.3 us
  Pallas kernels  88.4 us (98%)
  local copies, waits for them, and re-layouts  1.87 us (2%)
    pallas_call x1, Pallas kernels, layer(): pl.pallas_call(layer_kernel, out_shape=jax.ShapeDtypeStruct((length, 256)...  88.4 us
    unnamed x1, local copies, waits for them, and re-layouts  1.87 us

profile of v8, /device:TPU:1, one launch (start us, length us, event | category | flops | bytes accessed | tf_op | source)
XLA Modules:
  0.0 90.3 jit_solution(13341039078194847005)
XLA Ops:
  0.0 88.4 %layer.1 = bf16[1024,256]{1,0:T(8,128)(2,1)} custom-call(f32[2,2,1024]{2,1,0:T(2,128)} %bitcast.15, f32[2,2,1024]{2,1,0:T(2,128)} %bitcast.16, f32[4,2,128]{2,1,0:T(2,128)} %hbm_head.1, f32[4,2,128]{2,1,0:T(2,128)} %hbm_taps1.1, f32[4,2,64]{2,1,0:T(2,128)} %hbm_taps2.1, f32[2,128]{1,0:T(2,128)} %hbm_gain.1, f32[1,2048]{1,0:T(1,128)} %bitcast.17, ...), custom_call_target="tpu_custom_call" | custom-call | flops 12000000000 | bytes 8000000 | tf_op jit(solution)/shard_map/layer/pallas_call | solution.py:715
  88.4 1.9 %copy.21 = bf16[1024,256]{1,0:T(8,128)(2,1)} copy(bf16[1024,256]{1,0:T(8,128)(2,1)} %layer.1) | data formatting | bytes 1048576
